TPU v7x, 32 devices: a whole 2x2x4 slice. The times are simulated.
32 devices in a mesh: grp: 2 (over y), ep: 4 (over z), tp: 4 (over x, core).
Axes of the slice: x: 2, y: 2, z: 4, core: 2. Of those that a mesh axis runs over, the one named last changes fastest.
Arguments:
- tokens: bfloat16 [4096, 2048], P(('grp', 'ep', 'tp')), parts along dimension 0, may hold values from -6 to 6
- norm_gain: float32 [2048], replicated, may hold values from 0.1 to 1.9
- route_ids: int32 [4096, 2], P(('grp', 'ep', 'tp')), parts along dimension 0, may hold values from 0 to 15, all different within a row; in each aligned block of 128 rows (0 to 127, 128 to 255, ...) at most 24 rows name the same one
- route_weights: float32 [4096, 2], P(('grp', 'ep', 'tp')), parts along dimension 0, may hold values from 0.1 to 0.9
- w_gate: bfloat16 [16, 2048, 512], P(('ep', 'tp')), may hold values from -0.125 to 0.125
- w_up: bfloat16 [16, 2048, 512], P(('ep', 'tp')), may hold values from -0.125 to 0.125
- w_down: bfloat16 [16, 512, 2048], P(('ep', 'tp')), may hold values from -0.25 to 0.25
Outputs:
- mixed: bfloat16 [4096, 2048], P(('grp', 'ep', 'tp')), parts along dimension 0
There are 2 independent parts, one for each index of `grp`. A program takes and returns all parts, laid end to end along the dimension named above; an argument that names none is the same for every part. Nothing has to cross between parts.
Inputs may be any that keep to these rules, and one draw needn't show every extreme that they name: `route_ids`: each token names 2 different experts. Among the tokens of one device (aligned blocks of 128 tokens) no expert is named more than 24 times, a bound that some block reaches.
All inputs are finite; a program needn't handle non-finite values.
Results may differ from a plain program's by a relative error of at most 0.0071.
Values may be sent and summed in bfloat16 or wider, within the bound.
A program may use at most 64 MiB of HBM per device.

v0:
```python
import functools

import jax
import jax.numpy as jnp
from jax import lax
from jax.experimental import pallas as pl
from jax.experimental.pallas import tpu as pltpu
from jax.sharding import PartitionSpec as P

MESH = pl.DeviceIdType.MESH


def plain(tokens, norm_gain, route_ids, route_weights, w_gate, w_up, w_down):
    tok_rows, model_width = tokens.shape
    top_count = route_ids.shape[1]
    ep_count = lax.axis_size("ep")
    tp_count = lax.axis_size("tp")
    experts = ep_count * tp_count
    capacity = 3 * tok_rows * top_count // (2 * experts)
    values = tokens.astype(jnp.float32)
    normed = (
        values * lax.rsqrt(jnp.mean(values * values, axis=-1, keepdims=True) + 1e-06) * norm_gain
    ).astype(jnp.bfloat16)
    flat_ids = route_ids.reshape(-1)
    onehot = (flat_ids[:, None] == jnp.arange(experts, dtype=jnp.int32)[None, :]).astype(jnp.int32)
    slot_index = jnp.sum((jnp.cumsum(onehot, axis=0) - onehot) * onehot, axis=-1)
    token_of = jnp.arange(tok_rows * top_count, dtype=jnp.int32) // top_count
    buffer = jnp.zeros((experts, capacity, model_width), jnp.bfloat16)
    buffer = buffer.at[flat_ids, slot_index].set(normed[token_of])
    received = lax.all_to_all(buffer, ("ep", "tp"), split_axis=0, concat_axis=0, tiled=True)
    flat_rows = received.reshape(-1, model_width)
    gate_act = jnp.dot(flat_rows, w_gate[0], preferred_element_type=jnp.float32)
    up_act = jnp.dot(flat_rows, w_up[0], preferred_element_type=jnp.float32)
    hidden = (jax.nn.silu(gate_act) * up_act).astype(jnp.bfloat16)
    result = jnp.dot(hidden, w_down[0], preferred_element_type=jnp.float32).astype(jnp.bfloat16)
    returned = lax.all_to_all(
        result.reshape(received.shape), ("ep", "tp"), split_axis=0, concat_axis=0, tiled=True
    )
    picked = (
        returned[flat_ids, slot_index].reshape(tok_rows, top_count, model_width).astype(jnp.float32)
    )
    return jnp.sum(picked * route_weights[:, :, None], axis=1).astype(jnp.bfloat16)


def flipped(index, bits):
    bit = 1
    while bit <= bits:
        if bits & bit:
            index = index + (1 - 2 * ((index // bit) % 2)) * bit
        bit *= 2
    return index


PIECES = 4


def kernel(
    ep_count, tp_count, cap,
    x_hbm, gain_ref, ids_ref, wts_ref, wg_hbm, wu_hbm, wd_hbm, out_hbm,
    x_ref, out_ref, io_sem,
    normed, meta, share_hi, share_lo, nsend, nrecv, nres, nback,
    rblock, rmeta, rpick, rshare_hi, rshare_lo, fsend, frecv, fres, rback, rsend, farback,
    wg, wu, wd, acc,
    w_sem, dense_s, dense_r, meta_s, meta_r, near_s, near_r, nret_s, nret_r,
    far_s, far_r, fret_s, fret_r, final_s, final_r,
):
    ep, tp, grp = lax.axis_index("ep"), lax.axis_index("tp"), lax.axis_index("grp")
    rows, width = x_ref.shape
    part_w = width // PIECES
    top = ids_ref.shape[0]
    experts = ep_count * tp_count
    near = 2 * tp_count
    me = ep * tp_count + tp
    boundary = (ep + ep // 2) % 2
    wave_of_me = 1 - boundary
    own_relay, other_relay = 1 + ep // 2, 2 - ep // 2
    is_boundary, is_end = boundary == 1, boundary == 0

    def at(plane, j):
        return (grp, plane, flipped(tp, j))

    def remote(src, dst, s_sem, r_sem, target):
        return pltpu.make_async_remote_copy(
            src_ref=src, dst_ref=dst, send_sem=s_sem, recv_sem=r_sem,
            device_id=target, device_id_type=MESH,
        )

    barrier = pltpu.get_barrier_semaphore()

    def greet(target):
        pl.semaphore_signal(barrier, inc=1, device_id=target, device_id_type=MESH)

    greet(at(flipped(ep, 2), 0))

    @pl.when(is_boundary)
    def _():
        greet(at(flipped(ep, 3), 0))

    for g in range(near - 1, 0, -1):
        greet(at(flipped(ep, g // tp_count), g % tp_count))
    fetch = pltpu.make_async_copy(x_hbm, x_ref, io_sem.at[0])
    fetch.start()
    loads = [
        pltpu.make_async_copy(src.at[0], dst, w_sem.at[i])
        for i, (src, dst) in enumerate(((wg_hbm, wg), (wu_hbm, wu), (wd_hbm, wd)))
    ]
    for load in loads:
        load.start()

    planes = [ep, flipped(ep, 1)]
    dense = [
        remote(normed.at[c], rblock.at[wave_of_me, c], dense_s.at[c], dense_r.at[wave_of_me, c],
               at(other_relay, 0))
        for c in range(PIECES)
    ]
    meta_copy = remote(meta, rmeta.at[wave_of_me], meta_s.at[0], meta_r.at[wave_of_me],
                       at(other_relay, 0))
    stores = [
        pltpu.make_async_copy(
            out_ref.at[:, pl.ds(c * part_w, part_w)], out_hbm.at[:, pl.ds(c * part_w, part_w)],
            io_sem.at[1 + c])
        for c in range(PIECES)
    ]
    near_out = [
        remote(nsend.at[g], nrecv.at[g], near_s.at[g], near_r.at[g],
               at(planes[g // tp_count], g % tp_count))
        for g in range(near)
    ]
    near_ret = [
        remote(nres.at[g], nback.at[g], nret_s.at[g], nret_r.at[g],
               at(planes[g // tp_count], g % tp_count))
        for g in range(near)
    ]
    far_out, far_ret, final = {}, {}, {}
    for v in range(2):
        for c in range(PIECES):
            for i in range(near):
                far_out[v, c, i] = remote(
                    fsend.at[v, c, i], frecv.at[v, c, i % tp_count], far_s.at[v, c, i],
                    far_r.at[v, c, i % tp_count], at(planes[i // tp_count], i % tp_count))
            for j in range(tp_count):
                place = wave_of_me * tp_count + j
                far_ret[v, c, j] = remote(
                    fres.at[v, c, j], rback.at[v, c, place], fret_s.at[v, c, j],
                    fret_r.at[v, c, place], at(own_relay, j))
            final[v, c] = remote(rsend.at[v, c], farback.at[c], final_s.at[v, c], final_r.at[c],
                                 at(flipped(ep, 3 - v), 0))

    down = lax.broadcasted_iota(jnp.int32, (rows, rows), 0)
    across = lax.broadcasted_iota(jnp.int32, (rows, rows), 1)

    expert_of = lax.broadcasted_iota(jnp.int32, (experts, rows), 0) ^ me
    ids, wts = ids_ref[...], wts_ref[...]
    named = jnp.zeros((experts, rows), jnp.float32)
    weight = jnp.zeros((experts, rows), jnp.float32)
    for k in range(top):
        match = ids[k:k + 1] == expert_of
        named = named + jnp.where(match, 1.0, 0.0)
        weight = weight + jnp.where(match, wts[k:k + 1], 0.0)
    earlier = jnp.where(down < across, 1.0, 0.0).astype(jnp.bfloat16)
    rank = jnp.dot(named.astype(jnp.bfloat16), earlier, preferred_element_type=jnp.float32)
    rank = jnp.where(named > 0.5, rank, -1.0)
    meta[0:near] = rank[near:]
    meta[near:] = weight[near:]

    fetch.wait()
    values = x_ref[...].astype(jnp.float32)
    rows_normed = (
        values
        * lax.rsqrt(jnp.mean(values * values, axis=-1, keepdims=True) + 1e-06)
        * gain_ref[...]
    ).astype(jnp.bfloat16)
    for c in range(PIECES):
        normed[c] = rows_normed[:, c * part_w:(c + 1) * part_w]

    def onehots(rank, weight):
        slot = lax.broadcasted_iota(jnp.int32, (near, cap, rows), 1).astype(jnp.float32)
        taken = rank[:, None, :] == slot
        pick = jnp.where(taken, 1.0, 0.0).reshape(near * cap, rows).astype(jnp.bfloat16)
        share = jnp.where(taken, weight[:, None, :], 0.0).reshape(near * cap, rows)
        high = share.astype(jnp.bfloat16)
        return pick, high, (share - high.astype(jnp.float32)).astype(jnp.bfloat16)

    pl.semaphore_wait(barrier, near + boundary)

    @pl.when(is_boundary)
    def _():
        meta_copy.start()
        for c in range(PIECES):
            dense[c].start()

    pick, high, low = onehots(rank[:near], weight[:near])
    share_hi[...] = high
    share_lo[...] = low

    def pack_near(p):
        packed = jnp.dot(
            pick[p * tp_count * cap:(p + 1) * tp_count * cap], rows_normed,
            preferred_element_type=jnp.float32,
        ).astype(jnp.bfloat16).reshape(tp_count, cap, width)
        for j in range(tp_count):
            g = p * tp_count + j
            if g:
                nsend[g] = packed[j]
            else:
                nrecv[0] = packed[0]
        for j in range(tp_count):
            if p or j:
                near_out[p * tp_count + j].start()

    pack_near(1)

    @pl.when(is_end)
    def _():
        meta_copy.start()
        for c in range(PIECES):
            dense[c].start()

    pack_near(0)

    def hidden_of(gate_act, up_act):
        return (gate_act / (1.0 + jnp.exp(-gate_act)) * up_act).astype(jnp.bfloat16)

    def dot(a, b):
        return jnp.dot(a, b, preferred_element_type=jnp.float32)

    def expert_near(p):
        base = p * tp_count
        for g in range(base, base + tp_count):
            if g:
                near_out[g].wait_recv()
        block = nrecv[base:base + tp_count].reshape(tp_count * cap, width)
        hidden = hidden_of(dot(block, wg[...]), dot(block, wu[...]))
        result = dot(hidden, wd[...]).astype(jnp.bfloat16).reshape(tp_count, cap, width)
        for j in range(tp_count):
            if p or j:
                nres[base + j] = result[j]
            else:
                nback[0] = result[0]
        if p == 0:
            for j in range(1, tp_count):
                near_ret[j].start()

    def relay_out(v, c):
        @pl.when(is_boundary)
        def _():
            if c == 0:
                remote(meta, rmeta.at[v], meta_s.at[0], meta_r.at[v], at(other_relay, 0)).wait_recv()
                ranks, weights = rmeta[v, 0:near], rmeta[v, near:]
                if v == 0:
                    ranks = jnp.concatenate([ranks[tp_count:], ranks[:tp_count]], axis=0)
                    weights = jnp.concatenate([weights[tp_count:], weights[:tp_count]], axis=0)
                rp, rh, rl = onehots(ranks, weights)
                rpick[v] = rp
                rshare_hi[v] = rh
                rshare_lo[v] = rl
            remote(normed.at[c], rblock.at[v, c], dense_s.at[c], dense_r.at[v, c],
                   at(other_relay, 0)).wait_recv()
            packed = dot(rpick[v], rblock[v, c]).astype(jnp.bfloat16).reshape(near, cap, part_w)
            frecv[v, c, 0] = packed[0]
            for i in range(1, near):
                fsend[v, c, i] = packed[i]
            for i in list(range(tp_count, near)) + list(range(1, tp_count)):
                far_out[v, c, i].start()

    def expert_far(v):
        gate_act = up_act = None
        for c in range(PIECES):
            for j in range(1, tp_count):
                far_out[v, c, j].wait_recv()

            @pl.when(is_end)
            def _():
                far_out[v, c, tp_count].wait_recv()

            block = frecv[v, c].reshape(tp_count * cap, part_w)
            more_gate = dot(block, wg[c * part_w:(c + 1) * part_w])
            more_up = dot(block, wu[c * part_w:(c + 1) * part_w])
            gate_act = more_gate if c == 0 else gate_act + more_gate
            up_act = more_up if c == 0 else up_act + more_up
        hidden = hidden_of(gate_act, up_act)
        for c in range(PIECES):
            result = dot(hidden, wd[:, c * part_w:(c + 1) * part_w])
            result = result.astype(jnp.bfloat16).reshape(tp_count, cap, part_w)
            fres[v, c] = result
            for j in range(1, tp_count):
                far_ret[v, c, j].start()

            @pl.when(is_end)
            def _():
                far_ret[v, c, 0].start()

            @pl.when(is_boundary)
            def _():
                rback[v, c, 0] = fres[v, c, 0]

    def combine(high, low, block):
        total = None
        for comb in (high, low):
            term = lax.dot_general(
                comb, block, (((0,), (0,)), ((), ())), preferred_element_type=jnp.float32
            )
            total = term if total is None else total + term
        return total

    def relay_back(v, c):
        @pl.when(is_boundary)
        def _():
            for i in range(1, near):
                remote(fres.at[v, c, 0], rback.at[v, c, i], fret_s.at[v, c, 0],
                       fret_r.at[v, c, i], at(own_relay, 1)).wait_recv()
            block = rback[v, c].reshape(near * cap, part_w)
            rsend[v, c] = combine(rshare_hi[v], rshare_lo[v], block).astype(jnp.bfloat16)
            final[v, c].start()

    for load in loads:
        load.wait()
    def return_near(cond, js):
        @pl.when(cond)
        def _():
            for j in js:
                near_ret[tp_count + j].start()

    def return_near(cond, js):
        @pl.when(cond)
        def _():
            for j in js:
                near_ret[tp_count + j].start()

    expert_near(0)
    relay_out(0, 0)
    expert_near(1)
    return_near(is_end, range(tp_count))
    for c in range(1, PIECES):
        relay_out(0, c)
    expert_far(0)
    for c in range(PIECES):
        relay_out(1, c)
    return_near(is_boundary, range(tp_count))
    for c in range(PIECES):
        relay_back(0, c)
    expert_far(1)
    pass

    for g in range(1, near):
        near_ret[g].wait_recv()
    acc[...] = combine(share_hi[...], share_lo[...], nback[...].reshape(near * cap, width))
    for c in range(PIECES):
        relay_back(1, c)
    for c in range(PIECES):
        final[0, c].wait_recv()
        part = acc[:, c * part_w:(c + 1) * part_w] + farback[c].astype(jnp.float32)
        out_ref[:, c * part_w:(c + 1) * part_w] = part.astype(out_ref.dtype)
        stores[c].start()

    for store in stores:
        store.wait()
    meta_copy.wait_send()
    for copy in dense + near_out[1:] + near_ret[1:]:
        copy.wait_send()
    for v in range(2):
        for c in range(PIECES):
            for j in range(1, tp_count):
                far_ret[v, c, j].wait_send()

    @pl.when(is_end)
    def _():
        for v in range(2):
            for c in range(PIECES):
                far_ret[v, c, 0].wait_send()

    @pl.when(is_boundary)
    def _():
        for v in range(2):
            for c in range(PIECES):
                for i in range(1, near):
                    far_out[v, c, i].wait_send()
                final[v, c].wait_send()


def fused(ep_count, tp_count, tokens, norm_gain, route_ids, route_weights, w_gate, w_up, w_down):
    rows, width = tokens.shape
    hidden = w_gate.shape[2]
    experts = ep_count * tp_count
    near = 2 * tp_count
    cap = 3 * rows * route_ids.shape[1] // (2 * experts)
    part_w = width // PIECES
    vmem = pl.BlockSpec(memory_space=pltpu.VMEM)
    hbm = pl.BlockSpec(memory_space=pl.ANY)

    def b16(*shape):
        return pltpu.VMEM(shape, jnp.bfloat16)

    def sems(*shape):
        return pltpu.SemaphoreType.DMA(shape)

    return pl.pallas_call(
        functools.partial(kernel, ep_count, tp_count, cap),
        out_shape=jax.ShapeDtypeStruct((rows, width), tokens.dtype),
        in_specs=[hbm] + [vmem] * 3 + [hbm] * 3,
        out_specs=hbm,
        scratch_shapes=[
            b16(rows, width), b16(rows, width), sems(1 + PIECES),
            b16(PIECES, rows, part_w), pltpu.VMEM((2 * near, rows), jnp.float32),
            b16(near * cap, rows), b16(near * cap, rows),
            *[b16(near, cap, width)] * 4,
            b16(2, PIECES, rows, part_w), pltpu.VMEM((2, 2 * near, rows), jnp.float32),
            *[b16(2, near * cap, rows)] * 3,
            b16(2, PIECES, near, cap, part_w),
            b16(2, PIECES, tp_count, cap, part_w),
            b16(2, PIECES, tp_count, cap, part_w),
            b16(2, PIECES, near, cap, part_w),
            b16(2, PIECES, rows, part_w), b16(PIECES, rows, part_w),
            b16(width, hidden), b16(width, hidden), b16(hidden, width),
            pltpu.VMEM((rows, width), jnp.float32),
            sems(3), sems(PIECES), sems(2, PIECES), sems(1), sems(2),
            sems(near), sems(near), sems(near), sems(near),
            sems(2, PIECES, near), sems(2, PIECES, tp_count),
            sems(2, PIECES, tp_count), sems(2, PIECES, near),
            sems(2, PIECES), sems(PIECES),
        ],
        compiler_params=pltpu.CompilerParams(
            collective_id=0, has_side_effects=True, vmem_limit_bytes=56 * 1024 * 1024
        ),
    )(tokens, norm_gain.reshape(1, width), route_ids.T, route_weights.T, w_gate, w_up, w_down)


def solution(mesh):
    ep_count, tp_count = mesh.shape["ep"], mesh.shape["tp"]

    def on_device(*args):
        rows, experts = args[0].shape[0], ep_count * tp_count
        cap = 3 * rows * args[2].shape[1] // (2 * experts)
        if ep_count != 4 or tp_count != 4 or cap % 8 or rows % 128 or args[0].shape[1] % 256:
            return plain(*args)
        return fused(ep_count, tp_count, *args)

    return jax.shard_map(
        on_device,
        mesh=mesh,
        in_specs=(
            P(("grp", "ep", "tp"), None),
            P(),
            P(("grp", "ep", "tp"), None),
            P(("grp", "ep", "tp"), None),
            P(("ep", "tp"), None, None),
            P(("ep", "tp"), None, None),
            P(("ep", "tp"), None, None),
        ),
        out_specs=P(("grp", "ep", "tp"), None),
        check_vma=False,
    )
```

profile of v0, /device:TPU:0, one launch (start us, length us, event | category | flops | bytes accessed | tf_op | source)
XLA Modules:
  0.0 73.6 jit_solution(17049074544683762942)
XLA Ops:
  0.0 71.7 %shard_map.73 = bf16[128,2048]{1,0:T(8,128)(2,1)} custom-call(bf16[128,2048]{1,0:T(8,128)(2,1)} %x_hbm.1, f32[1,2048]{1,0:T(1,128)} %bitcast.3, s32[2,128]{1,0:T(2,128)} %bitcast.4, f32[2,128]{1,0:T(2,128)} %bitcast.5, bf16[1,2048,512]{2,1,0:T(8,128)(2,1)} %wg_hbm.1, bf16[1,2048,512]{2,1,0:T(8,128)(2,1)} %wu_hbm.1, bf16[1,512,2048]{2,1,0:T(8,128)(2,1)} %wd_hbm.1), custom_call_target="tpu_custom_call" | custom-call | tf_op jit(solution)/shard_map/pallas_call | solution.py:397
  71.7 1.9 %copy.9 = bf16[128,2048]{1,0:T(8,128)(2,1)} copy(bf16[128,2048]{1,0:T(8,128)(2,1)} %shard_map.73) | data formatting | bytes 1048576
where the time goes:
time: 73.8 us; the launch traced here: 73.6 us
  Pallas kernels  71.7 us (97%)
  local copies, waits for them, and re-layouts  1.88 us (3%)
    pallas_call x1, Pallas kernels, fused(): pl.pallas_call(functools.partial(kernel, ep_count, tp_count, cap), out_sh...  71.7 us
    unnamed x1, local copies, waits for them, and re-layouts  1.88 us

commit v1 on v0

--- a/solution.py
+++ b/solution.py
@@ -52,6 +52,7 @@
 
 
 PIECES = 4
+EARLY = 4
 
 
 def kernel(
@@ -59,10 +60,11 @@
     x_hbm, gain_ref, ids_ref, wts_ref, wg_hbm, wu_hbm, wd_hbm, out_hbm,
     x_ref, out_ref, io_sem,
     normed, meta, share_hi, share_lo, nsend, nrecv, nres, nback,
+    eblock, emeta, epick, esend,
     rblock, rmeta, rpick, rshare_hi, rshare_lo, fsend, frecv, fres, rback, rsend, farback,
-    wg, wu, wd, acc,
-    w_sem, dense_s, dense_r, meta_s, meta_r, near_s, near_r, nret_s, nret_r,
-    far_s, far_r, fret_s, fret_r, final_s, final_r,
+    wg, wu, wd, acc, gate_acc, up_acc,
+    w_sem, dense_s, fwd_s, edense_r, dense_r, meta_s, emeta_r, meta_r, near_s, near_r,
+    eout_s, nret_s, nret_r, far_s, far_r, fret_s, fret_r, final_s, final_r,
 ):
     ep, tp, grp = lax.axis_index("ep"), lax.axis_index("tp"), lax.axis_index("grp")
     rows, width = x_ref.shape
@@ -72,8 +74,8 @@
     near = 2 * tp_count
     me = ep * tp_count + tp
     boundary = (ep + ep // 2) % 2
-    wave_of_me = 1 - boundary
-    own_relay, other_relay = 1 + ep // 2, 2 - ep // 2
+    place_of_me = (1 - boundary) * tp_count
+    own_relay = 1 + ep // 2
     is_boundary, is_end = boundary == 1, boundary == 0
 
     def at(plane, j):
@@ -107,14 +109,26 @@
     for load in loads:
         load.start()
 
-    planes = [ep, flipped(ep, 1)]
+    partner, across_mid = flipped(ep, 1), flipped(ep, 3)
+    planes = [ep, partner]
     dense = [
-        remote(normed.at[c], rblock.at[wave_of_me, c], dense_s.at[c], dense_r.at[wave_of_me, c],
-               at(other_relay, 0))
+        remote(normed.at[c], rblock.at[0, c], dense_s.at[c], dense_r.at[0, c], at(across_mid, 0))
         for c in range(PIECES)
     ]
-    meta_copy = remote(meta, rmeta.at[wave_of_me], meta_s.at[0], meta_r.at[wave_of_me],
-                       at(other_relay, 0))
+    forward = [
+        remote(eblock.at[c], rblock.at[1, c], fwd_s.at[c], dense_r.at[1, c], at(across_mid, 0))
+        for c in range(PIECES)
+    ]
+    edense = [
+        remote(normed.at[c], eblock.at[c], dense_s.at[c], edense_r.at[c], at(partner, 0))
+        for c in range(PIECES)
+    ]
+    far_meta = pl.ds(0, 2 * near)
+    meta_copy = remote(meta.at[far_meta], rmeta.at[0], meta_s.at[0], meta_r.at[0],
+                       at(across_mid, 0))
+    meta_forward = remote(emeta.at[far_meta], rmeta.at[1], meta_s.at[1], meta_r.at[1],
+                          at(across_mid, 0))
+    emeta_copy = remote(meta, emeta, meta_s.at[0], emeta_r.at[0], at(partner, 0))
     stores = [
         pltpu.make_async_copy(
             out_ref.at[:, pl.ds(c * part_w, part_w)], out_hbm.at[:, pl.ds(c * part_w, part_w)],
@@ -126,6 +140,11 @@
                at(planes[g // tp_count], g % tp_count))
         for g in range(near)
     ]
+    eout = [
+        remote(esend.at[j], nrecv.at[tp_count + j], eout_s.at[j], near_r.at[tp_count + j],
+               at(ep, j))
+        for j in range(tp_count)
+    ]
     near_ret = [
         remote(nres.at[g], nback.at[g], nret_s.at[g], nret_r.at[g],
                at(planes[g // tp_count], g % tp_count))
@@ -139,7 +158,7 @@
                     fsend.at[v, c, i], frecv.at[v, c, i % tp_count], far_s.at[v, c, i],
                     far_r.at[v, c, i % tp_count], at(planes[i // tp_count], i % tp_count))
             for j in range(tp_count):
-                place = wave_of_me * tp_count + j
+                place = place_of_me + j
                 far_ret[v, c, j] = remote(
                     fres.at[v, c, j], rback.at[v, c, place], fret_s.at[v, c, j],
                     fret_r.at[v, c, place], at(own_relay, j))
@@ -161,7 +180,8 @@
     rank = jnp.dot(named.astype(jnp.bfloat16), earlier, preferred_element_type=jnp.float32)
     rank = jnp.where(named > 0.5, rank, -1.0)
     meta[0:near] = rank[near:]
-    meta[near:] = weight[near:]
+    meta[near:2 * near] = weight[near:]
+    meta[2 * near:] = rank[:near]
 
     fetch.wait()
     values = x_ref[...].astype(jnp.float32)
@@ -173,10 +193,15 @@
     for c in range(PIECES):
         normed[c] = rows_normed[:, c * part_w:(c + 1) * part_w]
 
+    def pick_of(rank):
+        count = rank.shape[0]
+        slot = lax.broadcasted_iota(jnp.int32, (count, cap, rows), 1).astype(jnp.float32)
+        taken = rank[:, None, :] == slot
+        pick = jnp.where(taken, 1.0, 0.0).reshape(count * cap, rows).astype(jnp.bfloat16)
+        return taken, pick
+
     def onehots(rank, weight):
-        slot = lax.broadcasted_iota(jnp.int32, (near, cap, rows), 1).astype(jnp.float32)
-        taken = rank[:, None, :] == slot
-        pick = jnp.where(taken, 1.0, 0.0).reshape(near * cap, rows).astype(jnp.bfloat16)
+        taken, pick = pick_of(rank)
         share = jnp.where(taken, weight[:, None, :], 0.0).reshape(near * cap, rows)
         high = share.astype(jnp.bfloat16)
         return pick, high, (share - high.astype(jnp.float32)).astype(jnp.bfloat16)
@@ -189,47 +214,41 @@
         for c in range(PIECES):
             dense[c].start()
 
+    @pl.when(is_end)
+    def _():
+        emeta_copy.start()
+        for c in range(PIECES):
+            edense[c].start()
+
     pick, high, low = onehots(rank[:near], weight[:near])
     share_hi[...] = high
     share_lo[...] = low
 
+    def dot(a, b):
+        return jnp.dot(a, b, preferred_element_type=jnp.float32)
+
+    half = tp_count * cap
+
     def pack_near(p):
-        packed = jnp.dot(
-            pick[p * tp_count * cap:(p + 1) * tp_count * cap], rows_normed,
-            preferred_element_type=jnp.float32,
-        ).astype(jnp.bfloat16).reshape(tp_count, cap, width)
+        packed = dot(pick[p * half:(p + 1) * half], rows_normed)
+        packed = packed.astype(jnp.bfloat16).reshape(tp_count, cap, width)
         for j in range(tp_count):
-            g = p * tp_count + j
-            if g:
-                nsend[g] = packed[j]
+            if p or j:
+                nsend[p * tp_count + j] = packed[j]
             else:
                 nrecv[0] = packed[0]
         for j in range(tp_count):
             if p or j:
                 near_out[p * tp_count + j].start()
 
-    pack_near(1)
-
-    @pl.when(is_end)
-    def _():
-        meta_copy.start()
-        for c in range(PIECES):
-            dense[c].start()
-
-    pack_near(0)
-
     def hidden_of(gate_act, up_act):
         return (gate_act / (1.0 + jnp.exp(-gate_act)) * up_act).astype(jnp.bfloat16)
 
-    def dot(a, b):
-        return jnp.dot(a, b, preferred_element_type=jnp.float32)
-
-    def expert_near(p):
+    def expert_near(p, waits):
         base = p * tp_count
-        for g in range(base, base + tp_count):
-            if g:
-                near_out[g].wait_recv()
-        block = nrecv[base:base + tp_count].reshape(tp_count * cap, width)
+        for g in waits:
+            near_out[base + g].wait_recv()
+        block = nrecv[base:base + tp_count].reshape(half, width)
         hidden = hidden_of(dot(block, wg[...]), dot(block, wu[...]))
         result = dot(hidden, wd[...]).astype(jnp.bfloat16).reshape(tp_count, cap, width)
         for j in range(tp_count):
@@ -237,62 +256,71 @@
                 nres[base + j] = result[j]
             else:
                 nback[0] = result[0]
-        if p == 0:
+
+    def return_near(gs):
+        for g in gs:
+            near_ret[g].start()
+
+    def forward_end(c):
+        edense[c].wait_recv()
+        forward[c].start()
+
+    def end_meta():
+        emeta_copy.wait_recv()
+        meta_forward.start()
+        epick[...] = pick_of(emeta[2 * near + tp_count:])[1]
+
+    def pack_end():
+        for c in range(PIECES):
+            packed = dot(epick[...], eblock[c]).astype(jnp.bfloat16).reshape(tp_count, cap, part_w)
+            nrecv[tp_count, :, c * part_w:(c + 1) * part_w] = packed[0]
             for j in range(1, tp_count):
-                near_ret[j].start()
+                esend[j, :, c * part_w:(c + 1) * part_w] = packed[j]
+        for j in range(1, tp_count):
+            eout[j].start()
+
+    def relay_meta(v):
+        remote(meta.at[far_meta], rmeta.at[v], meta_s.at[0], meta_r.at[v],
+               at(across_mid, 0)).wait_recv()
+        ranks, weights = rmeta[v, 0:near], rmeta[v, near:]
+        if v == 0:
+            ranks = jnp.concatenate([ranks[tp_count:], ranks[:tp_count]], axis=0)
+            weights = jnp.concatenate([weights[tp_count:], weights[:tp_count]], axis=0)
+        rp, rh, rl = onehots(ranks, weights)
+        rpick[v] = rp
+        rshare_hi[v] = rh
+        rshare_lo[v] = rl
 
     def relay_out(v, c):
-        @pl.when(is_boundary)
-        def _():
-            if c == 0:
-                remote(meta, rmeta.at[v], meta_s.at[0], meta_r.at[v], at(other_relay, 0)).wait_recv()
-                ranks, weights = rmeta[v, 0:near], rmeta[v, near:]
-                if v == 0:
-                    ranks = jnp.concatenate([ranks[tp_count:], ranks[:tp_count]], axis=0)
-                    weights = jnp.concatenate([weights[tp_count:], weights[:tp_count]], axis=0)
-                rp, rh, rl = onehots(ranks, weights)
-                rpick[v] = rp
-                rshare_hi[v] = rh
-                rshare_lo[v] = rl
-            remote(normed.at[c], rblock.at[v, c], dense_s.at[c], dense_r.at[v, c],
-                   at(other_relay, 0)).wait_recv()
-            packed = dot(rpick[v], rblock[v, c]).astype(jnp.bfloat16).reshape(near, cap, part_w)
-            frecv[v, c, 0] = packed[0]
-            for i in range(1, near):
-                fsend[v, c, i] = packed[i]
-            for i in list(range(tp_count, near)) + list(range(1, tp_count)):
-                far_out[v, c, i].start()
-
-    def expert_far(v):
-        gate_act = up_act = None
-        for c in range(PIECES):
-            for j in range(1, tp_count):
-                far_out[v, c, j].wait_recv()
-
-            @pl.when(is_end)
-            def _():
-                far_out[v, c, tp_count].wait_recv()
-
-            block = frecv[v, c].reshape(tp_count * cap, part_w)
-            more_gate = dot(block, wg[c * part_w:(c + 1) * part_w])
-            more_up = dot(block, wu[c * part_w:(c + 1) * part_w])
-            gate_act = more_gate if c == 0 else gate_act + more_gate
-            up_act = more_up if c == 0 else up_act + more_up
-        hidden = hidden_of(gate_act, up_act)
+        remote(normed.at[c], rblock.at[v, c], dense_s.at[c], dense_r.at[v, c],
+               at(across_mid, 0)).wait_recv()
+        packed = dot(rpick[v], rblock[v, c]).astype(jnp.bfloat16).reshape(near, cap, part_w)
+        frecv[v, c, 0] = packed[0]
+        for i in range(1, near):
+            fsend[v, c, i] = packed[i]
+        for i in list(range(tp_count, near)) + list(range(1, tp_count)):
+            far_out[v, c, i].start()
+
+    def far_in(v, c, waits):
+        for j in waits:
+            far_out[v, c, j].wait_recv()
+        block = frecv[v, c].reshape(half, part_w)
+        more_gate = dot(block, wg[c * part_w:(c + 1) * part_w])
+        more_up = dot(block, wu[c * part_w:(c + 1) * part_w])
+        gate_acc[...] = more_gate if c == 0 else gate_acc[...] + more_gate
+        up_acc[...] = more_up if c == 0 else up_acc[...] + more_up
+
+    def far_result(v, at_relay):
+        hidden = hidden_of(gate_acc[...], up_acc[...])
         for c in range(PIECES):
             result = dot(hidden, wd[:, c * part_w:(c + 1) * part_w])
             result = result.astype(jnp.bfloat16).reshape(tp_count, cap, part_w)
-            fres[v, c] = result
-            for j in range(1, tp_count):
+            if at_relay:
+                rback[v, c, 0] = result[0]
+            for j in range(at_relay, tp_count):
+                fres[v, c, j] = result[j]
+            for j in range(at_relay, tp_count):
                 far_ret[v, c, j].start()
-
-            @pl.when(is_end)
-            def _():
-                far_ret[v, c, 0].start()
-
-            @pl.when(is_boundary)
-            def _():
-                rback[v, c, 0] = fres[v, c, 0]
 
     def combine(high, low, block):
         total = None
@@ -304,59 +332,95 @@
         return total
 
     def relay_back(v, c):
-        @pl.when(is_boundary)
-        def _():
-            for i in range(1, near):
-                remote(fres.at[v, c, 0], rback.at[v, c, i], fret_s.at[v, c, 0],
-                       fret_r.at[v, c, i], at(own_relay, 1)).wait_recv()
-            block = rback[v, c].reshape(near * cap, part_w)
-            rsend[v, c] = combine(rshare_hi[v], rshare_lo[v], block).astype(jnp.bfloat16)
-            final[v, c].start()
-
-    for load in loads:
-        load.wait()
-    def return_near(cond, js):
-        @pl.when(cond)
-        def _():
-            for j in js:
-                near_ret[tp_count + j].start()
-
-    def return_near(cond, js):
-        @pl.when(cond)
-        def _():
-            for j in js:
-                near_ret[tp_count + j].start()
-
-    expert_near(0)
-    relay_out(0, 0)
-    expert_near(1)
-    return_near(is_end, range(tp_count))
-    for c in range(1, PIECES):
-        relay_out(0, c)
-    expert_far(0)
-    for c in range(PIECES):
-        relay_out(1, c)
-    return_near(is_boundary, range(tp_count))
-    for c in range(PIECES):
-        relay_back(0, c)
-    expert_far(1)
-    pass
-
-    for g in range(1, near):
-        near_ret[g].wait_recv()
-    acc[...] = combine(share_hi[...], share_lo[...], nback[...].reshape(near * cap, width))
-    for c in range(PIECES):
-        relay_back(1, c)
-    for c in range(PIECES):
+        for i in range(1, near):
+            remote(fres.at[v, c, 0], rback.at[v, c, i], fret_s.at[v, c, 0],
+                   fret_r.at[v, c, i], at(own_relay, 1)).wait_recv()
+        block = rback[v, c].reshape(near * cap, part_w)
+        rsend[v, c] = combine(rshare_hi[v], rshare_lo[v], block).astype(jnp.bfloat16)
+        final[v, c].start()
+
+    def combine_near():
+        for g in range(1, near):
+            near_ret[g].wait_recv()
+        acc[...] = combine(share_hi[...], share_lo[...], nback[...].reshape(near * cap, width))
+
+    def finish(c):
         final[0, c].wait_recv()
         part = acc[:, c * part_w:(c + 1) * part_w] + farback[c].astype(jnp.float32)
         out_ref[:, c * part_w:(c + 1) * part_w] = part.astype(out_ref.dtype)
         stores[c].start()
 
+    others, everyone = range(1, tp_count), range(tp_count)
+    second = range(tp_count, near)
+    def weights_here():
+        for load in loads:
+            load.wait()
+
+    @pl.when(is_boundary)
+    def _():
+        pack_near(0)
+        pack_near(1)
+        relay_meta(0)
+        relay_out(0, 0)
+        weights_here()
+        expert_near(0, others)
+        return_near(others)
+        relay_out(0, 1)
+        end_meta()
+        forward_end(0)
+        forward_end(1)
+        relay_out(0, 2)
+        forward_end(2)
+        relay_out(0, 3)
+        forward_end(3)
+        pack_end()
+        relay_meta(1)
+        for c in range(3):
+            far_in(0, c, others)
+        relay_out(1, 0)
+        far_in(0, 3, others)
+        far_result(0, 1)
+        relay_out(1, 1)
+        expert_near(1, others)
+        relay_out(1, 2)
+        relay_back(0, 0)
+        relay_back(0, 1)
+        relay_out(1, 3)
+        return_near(second)
+        relay_back(0, 2)
+        for c in range(PIECES):
+            far_in(1, c, others)
+        far_result(1, 1)
+        relay_back(0, 3)
+        for c in range(PIECES):
+            relay_back(1, c)
+        combine_near()
+        for c in range(PIECES):
+            finish(c)
+
+    @pl.when(is_end)
+    def _():
+        pack_near(0)
+        weights_here()
+        expert_near(0, others)
+        return_near(others)
+        far_in(0, 0, everyone)
+        expert_near(1, everyone)
+        return_near(list(second)[:EARLY])
+        for c in range(1, PIECES):
+            far_in(0, c, everyone)
+        far_result(0, 0)
+        for c in range(PIECES):
+            far_in(1, c, everyone)
+        far_result(1, 0)
+        return_near(list(second)[EARLY:])
+        combine_near()
+        for c in range(PIECES):
+            finish(c)
+
     for store in stores:
         store.wait()
-    meta_copy.wait_send()
-    for copy in dense + near_out[1:] + near_ret[1:]:
+    for copy in dense + near_out[1:tp_count] + near_ret[1:]:
         copy.wait_send()
     for v in range(2):
         for c in range(PIECES):
@@ -365,12 +429,17 @@
 
     @pl.when(is_end)
     def _():
+        emeta_copy.wait_send()
         for v in range(2):
             for c in range(PIECES):
                 far_ret[v, c, 0].wait_send()
 
     @pl.when(is_boundary)
     def _():
+        meta_copy.wait_send()
+        meta_forward.wait_send()
+        for copy in forward + near_out[tp_count:] + eout[1:]:
+            copy.wait_send()
         for v in range(2):
             for c in range(PIECES):
                 for i in range(1, near):
@@ -391,6 +460,9 @@
     def b16(*shape):
         return pltpu.VMEM(shape, jnp.bfloat16)
 
+    def f32(*shape):
+        return pltpu.VMEM(shape, jnp.float32)
+
     def sems(*shape):
         return pltpu.SemaphoreType.DMA(shape)
 
@@ -401,10 +473,12 @@
         out_specs=hbm,
         scratch_shapes=[
             b16(rows, width), b16(rows, width), sems(1 + PIECES),
-            b16(PIECES, rows, part_w), pltpu.VMEM((2 * near, rows), jnp.float32),
+            b16(PIECES, rows, part_w), f32(3 * near, rows),
             b16(near * cap, rows), b16(near * cap, rows),
             *[b16(near, cap, width)] * 4,
-            b16(2, PIECES, rows, part_w), pltpu.VMEM((2, 2 * near, rows), jnp.float32),
+            b16(PIECES, rows, part_w), f32(3 * near, rows),
+            b16(tp_count * cap, rows), b16(tp_count, cap, width),
+            b16(2, PIECES, rows, part_w), f32(2, 2 * near, rows),
             *[b16(2, near * cap, rows)] * 3,
             b16(2, PIECES, near, cap, part_w),
             b16(2, PIECES, tp_count, cap, part_w),
@@ -412,9 +486,10 @@
             b16(2, PIECES, near, cap, part_w),
             b16(2, PIECES, rows, part_w), b16(PIECES, rows, part_w),
             b16(width, hidden), b16(width, hidden), b16(hidden, width),
-            pltpu.VMEM((rows, width), jnp.float32),
-            sems(3), sems(PIECES), sems(2, PIECES), sems(1), sems(2),
-            sems(near), sems(near), sems(near), sems(near),
+            f32(rows, width), f32(tp_count * cap, hidden), f32(tp_count * cap, hidden),
+            sems(3), sems(PIECES), sems(PIECES), sems(PIECES), sems(2, PIECES),
+            sems(2), sems(1), sems(2),
+            sems(near), sems(near), sems(tp_count), sems(near), sems(near),
             sems(2, PIECES, near), sems(2, PIECES, tp_count),
             sems(2, PIECES, tp_count), sems(2, PIECES, near),
             sems(2, PIECES), sems(PIECES),

time: 73.8 us -> 67.8 us (0.919)
  Pallas kernels: 71.7 us -> 65.7 us
    pallas_call x1, Pallas kernels: 71.7 us -> 65.7 us  [fused(): pl.pallas_call(functools.partial(kernel, ep_count, tp_count, cap), out_sh...]
where the time goes in v1:
time: 67.8 us; the launch traced here: 67.6 us
  Pallas kernels  65.7 us (97%)
  local copies, waits for them, and re-layouts  1.88 us (3%)
    pallas_call x1, Pallas kernels, fused(): pl.pallas_call(functools.partial(kernel, ep_count, tp_count, cap), out_sh...  65.7 us
    unnamed x1, local copies, waits for them, and re-layouts  1.88 us

profile of v1, /device:TPU:0, one launch (start us, length us, event | category | flops | bytes accessed | tf_op | source)
XLA Modules:
  0.0 67.6 jit_solution(15795263882031818443)
XLA Ops:
  0.0 65.7 %shard_map.73 = bf16[128,2048]{1,0:T(8,128)(2,1)} custom-call(bf16[128,2048]{1,0:T(8,128)(2,1)} %x_hbm.1, f32[1,2048]{1,0:T(1,128)} %bitcast.3, s32[2,128]{1,0:T(2,128)} %bitcast.4, f32[2,128]{1,0:T(2,128)} %bitcast.5, bf16[1,2048,512]{2,1,0:T(8,128)(2,1)} %wg_hbm.1, bf16[1,2048,512]{2,1,0:T(8,128)(2,1)} %wu_hbm.1, bf16[1,512,2048]{2,1,0:T(8,128)(2,1)} %wd_hbm.1), custom_call_target="tpu_custom_call" | custom-call | tf_op jit(solution)/shard_map/pallas_call | solution.py:469
  65.7 1.9 %copy.9 = bf16[128,2048]{1,0:T(8,128)(2,1)} copy(bf16[128,2048]{1,0:T(8,128)(2,1)} %shard_map.73) | data formatting | bytes 1048576

commit v2 on v1

--- a/solution.py
+++ b/solution.py
@@ -51,20 +51,21 @@
     return index
 
 
-PIECES = 4
-EARLY = 4
+PIECES = 8
+EARLY = 1
+GROUPS = ((0, 1), (1, 3), (3, 8))
 
 
 def kernel(
     ep_count, tp_count, cap,
-    x_hbm, gain_ref, ids_ref, wts_ref, wg_hbm, wu_hbm, wd_hbm, out_hbm,
-    x_ref, out_ref, io_sem,
+    x_hbm, gain_hbm, ids_hbm, wts_hbm, wg_hbm, wu_hbm, wd_hbm, out_ref,
+    x_ref, gain_ref, ids_ref, wts_ref, io_sem,
     normed, meta, share_hi, share_lo, nsend, nrecv, nres, nback,
     eblock, emeta, epick, esend,
     rblock, rmeta, rpick, rshare_hi, rshare_lo, fsend, frecv, fres, rback, rsend, farback,
     wg, wu, wd, acc, gate_acc, up_acc,
     w_sem, dense_s, fwd_s, edense_r, dense_r, meta_s, emeta_r, meta_r, near_s, near_r,
-    eout_s, nret_s, nret_r, far_s, far_r, fret_s, fret_r, final_s, final_r,
+    eout_s, lend_r, nret_s, nret_r, far_s, far_r, fret_s, fret_r, final_s, final_r,
 ):
     ep, tp, grp = lax.axis_index("ep"), lax.axis_index("tp"), lax.axis_index("grp")
     rows, width = x_ref.shape
@@ -100,27 +101,29 @@
 
     for g in range(near - 1, 0, -1):
         greet(at(flipped(ep, g // tp_count), g % tp_count))
-    fetch = pltpu.make_async_copy(x_hbm, x_ref, io_sem.at[0])
-    fetch.start()
+    fetches = [
+        pltpu.make_async_copy(src, dst, io_sem.at[i])
+        for i, (src, dst) in enumerate((
+            (x_hbm, x_ref), (gain_hbm, gain_ref), (ids_hbm, ids_ref), (wts_hbm, wts_ref)))
+    ]
+    for fetch in fetches:
+        fetch.start()
     loads = [
         pltpu.make_async_copy(src.at[0], dst, w_sem.at[i])
         for i, (src, dst) in enumerate(((wg_hbm, wg), (wu_hbm, wu), (wd_hbm, wd)))
     ]
-    for load in loads:
-        load.start()
-
     partner, across_mid = flipped(ep, 1), flipped(ep, 3)
     planes = [ep, partner]
     dense = [
-        remote(normed.at[c], rblock.at[0, c], dense_s.at[c], dense_r.at[0, c], at(across_mid, 0))
+        remote(normed.at[c], rblock.at[0, c], dense_s, dense_r.at[0, c], at(across_mid, 0))
         for c in range(PIECES)
     ]
     forward = [
-        remote(eblock.at[c], rblock.at[1, c], fwd_s.at[c], dense_r.at[1, c], at(across_mid, 0))
+        remote(eblock.at[c], rblock.at[1, c], fwd_s, dense_r.at[1, c], at(across_mid, 0))
         for c in range(PIECES)
     ]
     edense = [
-        remote(normed.at[c], eblock.at[c], dense_s.at[c], edense_r.at[c], at(partner, 0))
+        remote(normed.at[c], eblock.at[c], dense_s, edense_r.at[c], at(partner, 0))
         for c in range(PIECES)
     ]
     far_meta = pl.ds(0, 2 * near)
@@ -129,24 +132,26 @@
     meta_forward = remote(emeta.at[far_meta], rmeta.at[1], meta_s.at[1], meta_r.at[1],
                           at(across_mid, 0))
     emeta_copy = remote(meta, emeta, meta_s.at[0], emeta_r.at[0], at(partner, 0))
-    stores = [
-        pltpu.make_async_copy(
-            out_ref.at[:, pl.ds(c * part_w, part_w)], out_hbm.at[:, pl.ds(c * part_w, part_w)],
-            io_sem.at[1 + c])
-        for c in range(PIECES)
-    ]
     near_out = [
-        remote(nsend.at[g], nrecv.at[g], near_s.at[g], near_r.at[g],
+        remote(nsend.at[g], nrecv.at[g], near_s, near_r.at[g // tp_count],
                at(planes[g // tp_count], g % tp_count))
         for g in range(near)
     ]
+    side = tp_count // 2
     eout = [
-        remote(esend.at[j], nrecv.at[tp_count + j], eout_s.at[j], near_r.at[tp_count + j],
-               at(ep, j))
-        for j in range(tp_count)
+        remote(esend.at[j], nrecv.at[tp_count + j], eout_s, near_r.at[1], at(ep, j))
+        for j in range(side)
+    ]
+    lend = [
+        remote(nsend.at[tp_count + side + k], esend.at[k], near_s, lend_r, at(ep, side))
+        for k in range(side)
+    ]
+    pass_on = [
+        remote(esend.at[k], nrecv.at[tp_count + side + k], eout_s, near_r.at[1], at(partner, k))
+        for k in range(side)
     ]
     near_ret = [
-        remote(nres.at[g], nback.at[g], nret_s.at[g], nret_r.at[g],
+        remote(nres.at[g], nback.at[g], nret_s, nret_r,
                at(planes[g // tp_count], g % tp_count))
         for g in range(near)
     ]
@@ -155,20 +160,25 @@
         for c in range(PIECES):
             for i in range(near):
                 far_out[v, c, i] = remote(
-                    fsend.at[v, c, i], frecv.at[v, c, i % tp_count], far_s.at[v, c, i],
-                    far_r.at[v, c, i % tp_count], at(planes[i // tp_count], i % tp_count))
+                    fsend.at[v, c, i], frecv.at[v, c, i % tp_count], far_s,
+                    far_r.at[v, c], at(planes[i // tp_count], i % tp_count))
             for j in range(tp_count):
                 place = place_of_me + j
                 far_ret[v, c, j] = remote(
-                    fres.at[v, c, j], rback.at[v, c, place], fret_s.at[v, c, j],
-                    fret_r.at[v, c, place], at(own_relay, j))
-            final[v, c] = remote(rsend.at[v, c], farback.at[c], final_s.at[v, c], final_r.at[c],
+                    fres.at[v, c, j], rback.at[v, c, place], fret_s, fret_r.at[v, c],
+                    at(own_relay, j))
+            final[v, c] = remote(rsend.at[v, c], farback.at[c], final_s, final_r.at[c],
                                  at(flipped(ep, 3 - v), 0))
+
+    def drain(ref, sem):
+        pltpu.make_async_copy(ref, ref, sem).wait()
 
     down = lax.broadcasted_iota(jnp.int32, (rows, rows), 0)
     across = lax.broadcasted_iota(jnp.int32, (rows, rows), 1)
 
     expert_of = lax.broadcasted_iota(jnp.int32, (experts, rows), 0) ^ me
+    for fetch in fetches[2:]:
+        fetch.wait()
     ids, wts = ids_ref[...], wts_ref[...]
     named = jnp.zeros((experts, rows), jnp.float32)
     weight = jnp.zeros((experts, rows), jnp.float32)
@@ -183,7 +193,10 @@
     meta[near:2 * near] = weight[near:]
     meta[2 * near:] = rank[:near]
 
-    fetch.wait()
+    for fetch in fetches[:2]:
+        fetch.wait()
+    for load in loads:
+        load.start()
     values = x_ref[...].astype(jnp.float32)
     rows_normed = (
         values
@@ -237,17 +250,18 @@
                 nsend[p * tp_count + j] = packed[j]
             else:
                 nrecv[0] = packed[0]
-        for j in range(tp_count):
-            if p or j:
-                near_out[p * tp_count + j].start()
+        send_near(range(2) if p else range(1, tp_count), p)
+
+    def send_near(js, p=1):
+        for j in js:
+            near_out[p * tp_count + j].start()
 
     def hidden_of(gate_act, up_act):
         return (gate_act / (1.0 + jnp.exp(-gate_act)) * up_act).astype(jnp.bfloat16)
 
-    def expert_near(p, waits):
+    def expert_near(p, first):
         base = p * tp_count
-        for g in waits:
-            near_out[base + g].wait_recv()
+        drain(nrecv.at[pl.ds(base + first, tp_count - first)], near_r.at[p])
         block = nrecv[base:base + tp_count].reshape(half, width)
         hidden = hidden_of(dot(block, wg[...]), dot(block, wu[...]))
         result = dot(hidden, wd[...]).astype(jnp.bfloat16).reshape(tp_count, cap, width)
@@ -268,16 +282,28 @@
     def end_meta():
         emeta_copy.wait_recv()
         meta_forward.start()
-        epick[...] = pick_of(emeta[2 * near + tp_count:])[1]
+        epick[...] = pick_of(emeta[2 * near + tp_count:2 * near + tp_count + side])[1]
 
     def pack_end():
         for c in range(PIECES):
-            packed = dot(epick[...], eblock[c]).astype(jnp.bfloat16).reshape(tp_count, cap, part_w)
+            packed = dot(epick[...], eblock[c]).astype(jnp.bfloat16).reshape(side, cap, part_w)
             nrecv[tp_count, :, c * part_w:(c + 1) * part_w] = packed[0]
-            for j in range(1, tp_count):
+            for j in range(1, side):
                 esend[j, :, c * part_w:(c + 1) * part_w] = packed[j]
-        for j in range(1, tp_count):
+        for j in range(1, side):
             eout[j].start()
+
+    def pack_lend():
+        packed = dot(pick[half + side * cap:], rows_normed)
+        packed = packed.astype(jnp.bfloat16).reshape(tp_count - side, cap, width)
+        for k in range(side):
+            nsend[tp_count + side + k] = packed[k]
+            lend[k].start()
+
+    def send_lent():
+        drain(esend, lend_r)
+        for copy in pass_on:
+            copy.start()
 
     def relay_meta(v):
         remote(meta.at[far_meta], rmeta.at[v], meta_s.at[0], meta_r.at[v],
@@ -292,7 +318,7 @@
         rshare_lo[v] = rl
 
     def relay_out(v, c):
-        remote(normed.at[c], rblock.at[v, c], dense_s.at[c], dense_r.at[v, c],
+        remote(normed.at[c], rblock.at[v, c], dense_s, dense_r.at[v, c],
                at(across_mid, 0)).wait_recv()
         packed = dot(rpick[v], rblock[v, c]).astype(jnp.bfloat16).reshape(near, cap, part_w)
         frecv[v, c, 0] = packed[0]
@@ -301,9 +327,8 @@
         for i in list(range(tp_count, near)) + list(range(1, tp_count)):
             far_out[v, c, i].start()
 
-    def far_in(v, c, waits):
-        for j in waits:
-            far_out[v, c, j].wait_recv()
+    def far_in(v, c, first):
+        drain(frecv.at[v, c, pl.ds(first, tp_count - first)], far_r.at[v, c])
         block = frecv[v, c].reshape(half, part_w)
         more_gate = dot(block, wg[c * part_w:(c + 1) * part_w])
         more_up = dot(block, wu[c * part_w:(c + 1) * part_w])
@@ -312,15 +337,17 @@
 
     def far_result(v, at_relay):
         hidden = hidden_of(gate_acc[...], up_acc[...])
-        for c in range(PIECES):
-            result = dot(hidden, wd[:, c * part_w:(c + 1) * part_w])
-            result = result.astype(jnp.bfloat16).reshape(tp_count, cap, part_w)
-            if at_relay:
-                rback[v, c, 0] = result[0]
-            for j in range(at_relay, tp_count):
-                fres[v, c, j] = result[j]
-            for j in range(at_relay, tp_count):
-                far_ret[v, c, j].start()
+        for lo, hi in GROUPS:
+            result = dot(hidden, wd[:, lo * part_w:hi * part_w])
+            result = result.astype(jnp.bfloat16).reshape(tp_count, cap, (hi - lo) * part_w)
+            for c in range(lo, hi):
+                part = result[:, :, (c - lo) * part_w:(c - lo + 1) * part_w]
+                if at_relay:
+                    rback[v, c, 0] = part[0]
+                for j in range(at_relay, tp_count):
+                    fres[v, c, j] = part[j]
+                for j in range(at_relay, tp_count):
+                    far_ret[v, c, j].start()
 
     def combine(high, low, block):
         total = None
@@ -332,26 +359,23 @@
         return total
 
     def relay_back(v, c):
-        for i in range(1, near):
-            remote(fres.at[v, c, 0], rback.at[v, c, i], fret_s.at[v, c, 0],
-                   fret_r.at[v, c, i], at(own_relay, 1)).wait_recv()
+        drain(rback.at[v, c, pl.ds(1, near - 1)], fret_r.at[v, c])
         block = rback[v, c].reshape(near * cap, part_w)
         rsend[v, c] = combine(rshare_hi[v], rshare_lo[v], block).astype(jnp.bfloat16)
         final[v, c].start()
 
     def combine_near():
-        for g in range(1, near):
-            near_ret[g].wait_recv()
+        drain(nback.at[pl.ds(1, near - 1)], nret_r)
         acc[...] = combine(share_hi[...], share_lo[...], nback[...].reshape(near * cap, width))
 
     def finish(c):
         final[0, c].wait_recv()
         part = acc[:, c * part_w:(c + 1) * part_w] + farback[c].astype(jnp.float32)
         out_ref[:, c * part_w:(c + 1) * part_w] = part.astype(out_ref.dtype)
-        stores[c].start()
-
-    others, everyone = range(1, tp_count), range(tp_count)
+
+    others = range(1, tp_count)
     second = range(tp_count, near)
+
     def weights_here():
         for load in loads:
             load.wait()
@@ -361,37 +385,44 @@
         pack_near(0)
         pack_near(1)
         relay_meta(0)
-        relay_out(0, 0)
-        weights_here()
-        expert_near(0, others)
-        return_near(others)
-        relay_out(0, 1)
+        last = PIECES - 1
+        ahead = PIECES // 2
+        for c in range(ahead):
+            relay_out(0, c)
+            if c == 0:
+                weights_here()
+                expert_near(0, 1)
+                return_near(others)
         end_meta()
-        forward_end(0)
-        forward_end(1)
-        relay_out(0, 2)
-        forward_end(2)
-        relay_out(0, 3)
-        forward_end(3)
+        for c in range(ahead - 1):
+            forward_end(c)
+        for c in range(ahead, PIECES):
+            relay_out(0, c)
+            forward_end(c - 1)
+        forward_end(last)
+        send_near(range(2, tp_count))
         pack_end()
         relay_meta(1)
-        for c in range(3):
-            far_in(0, c, others)
+        for c in range(PIECES // 2):
+            far_in(0, c, 1)
         relay_out(1, 0)
-        far_in(0, 3, others)
+        for c in range(PIECES // 2, PIECES):
+            far_in(0, c, 1)
         far_result(0, 1)
-        relay_out(1, 1)
-        expert_near(1, others)
-        relay_out(1, 2)
+        for c in range(1, PIECES - 1):
+            relay_out(1, c)
         relay_back(0, 0)
+        relay_out(1, last)
         relay_back(0, 1)
-        relay_out(1, 3)
+        expert_near(1, 1)
         return_near(second)
         relay_back(0, 2)
-        for c in range(PIECES):
-            far_in(1, c, others)
+        relay_back(0, 3)
+        for c in range(4, PIECES):
+            far_in(1, 2 * c - 8, 1)
+            far_in(1, 2 * c - 7, 1)
+            relay_back(0, c)
         far_result(1, 1)
-        relay_back(0, 3)
         for c in range(PIECES):
             relay_back(1, c)
         combine_near()
@@ -401,50 +432,44 @@
     @pl.when(is_end)
     def _():
         pack_near(0)
+        pack_lend()
         weights_here()
-        expert_near(0, others)
+        expert_near(0, 1)
         return_near(others)
-        far_in(0, 0, everyone)
-        expert_near(1, everyone)
+        send_lent()
+        for c in range(PIECES):
+            far_in(0, c, 0)
+        far_result(0, 0)
+        expert_near(1, 0)
         return_near(list(second)[:EARLY])
-        for c in range(1, PIECES):
-            far_in(0, c, everyone)
-        far_result(0, 0)
-        for c in range(PIECES):
-            far_in(1, c, everyone)
+        for c in range(PIECES):
+            far_in(1, c, 0)
         far_result(1, 0)
         return_near(list(second)[EARLY:])
         combine_near()
         for c in range(PIECES):
             finish(c)
 
-    for store in stores:
-        store.wait()
-    for copy in dense + near_out[1:tp_count] + near_ret[1:]:
-        copy.wait_send()
-    for v in range(2):
-        for c in range(PIECES):
-            for j in range(1, tp_count):
-                far_ret[v, c, j].wait_send()
+    drain(normed, dense_s)
+    drain(nres.at[pl.ds(1, near - 1)], nret_s)
 
     @pl.when(is_end)
     def _():
-        emeta_copy.wait_send()
-        for v in range(2):
-            for c in range(PIECES):
-                far_ret[v, c, 0].wait_send()
+        drain(meta, meta_s.at[0])
+        drain(nsend.at[pl.ds(1, tp_count + side - 1)], near_s)
+        drain(esend, eout_s)
+        drain(fres, fret_s)
 
     @pl.when(is_boundary)
     def _():
-        meta_copy.wait_send()
-        meta_forward.wait_send()
-        for copy in forward + near_out[tp_count:] + eout[1:]:
-            copy.wait_send()
-        for v in range(2):
-            for c in range(PIECES):
-                for i in range(1, near):
-                    far_out[v, c, i].wait_send()
-                final[v, c].wait_send()
+        drain(meta.at[far_meta], meta_s.at[0])
+        drain(meta.at[far_meta], meta_s.at[1])
+        drain(eblock, fwd_s)
+        drain(nsend.at[pl.ds(1, near - 1)], near_s)
+        drain(esend.at[pl.ds(1, side - 1)], eout_s)
+        drain(fres.at[:, :, pl.ds(1, tp_count - 1)], fret_s)
+        drain(fsend.at[:, :, pl.ds(1, near - 1)], far_s)
+        drain(rsend, final_s)
 
 
 def fused(ep_count, tp_count, tokens, norm_gain, route_ids, route_weights, w_gate, w_up, w_down):
@@ -455,7 +480,7 @@
     cap = 3 * rows * route_ids.shape[1] // (2 * experts)
     part_w = width // PIECES
     vmem = pl.BlockSpec(memory_space=pltpu.VMEM)
-    hbm = pl.BlockSpec(memory_space=pl.ANY)
+    hbm = pl.BlockSpec(memory_space=pltpu.HBM)
 
     def b16(*shape):
         return pltpu.VMEM(shape, jnp.bfloat16)
@@ -466,18 +491,20 @@
     def sems(*shape):
         return pltpu.SemaphoreType.DMA(shape)
 
+    one = pltpu.SemaphoreType.DMA
     return pl.pallas_call(
         functools.partial(kernel, ep_count, tp_count, cap),
         out_shape=jax.ShapeDtypeStruct((rows, width), tokens.dtype),
-        in_specs=[hbm] + [vmem] * 3 + [hbm] * 3,
-        out_specs=hbm,
+        in_specs=[hbm] * 7,
+        out_specs=vmem,
         scratch_shapes=[
-            b16(rows, width), b16(rows, width), sems(1 + PIECES),
+            b16(rows, width), f32(1, width),
+            pltpu.VMEM(route_ids.shape[::-1], jnp.int32), f32(*route_weights.shape[::-1]), sems(4),
             b16(PIECES, rows, part_w), f32(3 * near, rows),
             b16(near * cap, rows), b16(near * cap, rows),
             *[b16(near, cap, width)] * 4,
             b16(PIECES, rows, part_w), f32(3 * near, rows),
-            b16(tp_count * cap, rows), b16(tp_count, cap, width),
+            b16(tp_count // 2 * cap, rows), b16(tp_count // 2, cap, width),
             b16(2, PIECES, rows, part_w), f32(2, 2 * near, rows),
             *[b16(2, near * cap, rows)] * 3,
             b16(2, PIECES, near, cap, part_w),
@@ -487,17 +514,18 @@
             b16(2, PIECES, rows, part_w), b16(PIECES, rows, part_w),
             b16(width, hidden), b16(width, hidden), b16(hidden, width),
             f32(rows, width), f32(tp_count * cap, hidden), f32(tp_count * cap, hidden),
-            sems(3), sems(PIECES), sems(PIECES), sems(PIECES), sems(2, PIECES),
-            sems(2), sems(1), sems(2),
-            sems(near), sems(near), sems(tp_count), sems(near), sems(near),
-            sems(2, PIECES, near), sems(2, PIECES, tp_count),
-            sems(2, PIECES, tp_count), sems(2, PIECES, near),
-            sems(2, PIECES), sems(PIECES),
+            sems(3), one, one, sems(PIECES), sems(2, PIECES),
+            sems(2), sems(1), sems(2), one, sems(2), one, one, one, one,
+            one, sems(2, PIECES), one, sems(2, PIECES), one, sems(PIECES),
         ],
         compiler_params=pltpu.CompilerParams(
-            collective_id=0, has_side_effects=True, vmem_limit_bytes=56 * 1024 * 1024
+            collective_id=0, has_side_effects=True, vmem_limit_bytes=32 * 1024 * 1024
         ),
-    )(tokens, norm_gain.reshape(1, width), route_ids.T, route_weights.T, w_gate, w_up, w_down)
+    )(*(
+        pltpu.with_memory_space_constraint(arg, pltpu.HBM)
+        for arg in (tokens, norm_gain.reshape(1, width), route_ids.T, route_weights.T,
+                    w_gate, w_up, w_down)
+    ))
 
 
 def solution(mesh):

time: 67.8 us -> 56.9 us (0.84)
  Pallas kernels: 65.7 us -> 55.9 us
  local copies, waits for them, and re-layouts: 1.88 us -> 0.8 us
    pallas_call x1, Pallas kernels: 65.7 us -> 55.9 us  [fused(): pl.pallas_call(functools.partial(kernel, ep_count, tp_count, cap), out_sh...]
    unnamed x1, local copies, waits for them, and re-layouts: 1.88 us -> 0.8 us
where the time goes in v2:
time: 56.9 us; the launch traced here: 56.7 us
  Pallas kernels  55.9 us (98%)
  local copies, waits for them, and re-layouts  0.8 us (1%)
    pallas_call x1, Pallas kernels, fused(): pl.pallas_call(functools.partial(kernel, ep_count, tp_count, cap), out_sh...  55.9 us

profile of v2, /device:TPU:0, one launch (start us, length us, event | category | flops | bytes accessed | tf_op | source)
XLA Modules:
  0.0 56.7 jit_solution(6942910751685545092)
XLA Ops:
  0.0 55.9 %shard_map.73 = bf16[128,2048]{1,0:T(8,128)(2,1)S(1)} custom-call(bf16[128,2048]{1,0:T(8,128)(2,1)} %x_hbm.1, f32[1,2048]{1,0:T(1,128)} %bitcast.3, s32[2,128]{1,0:T(2,128)} %bitcast.4, f32[2,128]{1,0:T(2,128)} %bitcast.5, bf16[1,2048,512]{2,1,0:T(8,128)(2,1)} %wg_hbm.1, bf16[1,2048,512]{2,1,0:T(8,128)(2,1)} %wu_hbm.1, bf16[1,512,2048]{2,1,0:T(8,128)(2,1)} %wd_hbm.1), custom_call_target="tpu_custom_call" | custom-call | tf_op jit(solution)/shard_map/pallas_call | solution.py:495
  55.9 0.8 %copy.9 = bf16[128,2048]{1,0:T(8,128)(2,1)} copy(bf16[128,2048]{1,0:T(8,128)(2,1)S(1)} %shard_map.73) | data formatting | bytes 1048576

commit v3 on v2

--- a/solution.py
+++ b/solution.py
@@ -53,7 +53,24 @@
 
 PIECES = 8
 EARLY = 1
+AHEAD = 3
+DIRECT = 2
 GROUPS = ((0, 1), (1, 3), (3, 8))
+DENSE_BY = (0, 2, 4, 6, 7, 8)
+EDENSE_BY = (0, 2, 4, 6, 8)
+FAR_BY = (0, 4, 6, 7, 8)
+BACK_BY = (0, 1, 2, 3, 4, 5, 6, 7, 8)
+HOP_BY = (DIRECT, 4, 6, 8)
+FINAL_BY = (0, 6, 7, 8)
+
+
+def span(edges, c):
+    g = max(i for i in range(len(edges) - 1) if edges[i] <= c)
+    return g, edges[g], edges[g + 1] - edges[g]
+
+
+def slot(edges, c):
+    return span(edges, c)[0]
 
 
 def kernel(
@@ -61,11 +78,11 @@
     x_hbm, gain_hbm, ids_hbm, wts_hbm, wg_hbm, wu_hbm, wd_hbm, out_ref,
     x_ref, gain_ref, ids_ref, wts_ref, io_sem,
     normed, meta, share_hi, share_lo, nsend, nrecv, nres, nback,
-    eblock, emeta, epick, esend,
+    eblock, emeta, epick, esend, hop,
     rblock, rmeta, rpick, rshare_hi, rshare_lo, fsend, frecv, fres, rback, rsend, farback,
     wg, wu, wd, acc, gate_acc, up_acc,
-    w_sem, dense_s, fwd_s, edense_r, dense_r, meta_s, emeta_r, meta_r, near_s, near_r,
-    eout_s, lend_r, nret_s, nret_r, far_s, far_r, fret_s, fret_r, final_s, final_r,
+    w_sem, ready, dense_s, fwd_s, edense_r, dense_r, meta_s, emeta_r, meta_r, near_s, near_r,
+    eout_s, lend_r, nret_s, nret_r, far_s, far_r, fret_s, fret_r, hop_s, hop_r, final_s, final_r,
 ):
     ep, tp, grp = lax.axis_index("ep"), lax.axis_index("tp"), lax.axis_index("grp")
     rows, width = x_ref.shape
@@ -78,6 +95,8 @@
     place_of_me = (1 - boundary) * tp_count
     own_relay = 1 + ep // 2
     is_boundary, is_end = boundary == 1, boundary == 0
+    is_first = ep < ep_count // 2
+    holds_back = jnp.logical_and(ep == ep_count // 2, tp % 2 == 0)
 
     def at(plane, j):
         return (grp, plane, flipped(tp, j))
@@ -93,14 +112,19 @@
     def greet(target):
         pl.semaphore_signal(barrier, inc=1, device_id=target, device_id_type=MESH)
 
-    greet(at(flipped(ep, 2), 0))
-
     @pl.when(is_boundary)
     def _():
         greet(at(flipped(ep, 3), 0))
-
-    for g in range(near - 1, 0, -1):
-        greet(at(flipped(ep, g // tp_count), g % tp_count))
+        for j in range(tp_count):
+            greet(at(flipped(ep, 1), j))
+
+    @pl.when(jnp.logical_and(is_end, is_first))
+    def _():
+        for j in range(tp_count):
+            greet(at(flipped(ep, 1), j))
+
+    for j in range(1, tp_count):
+        greet(at(ep, j))
     fetches = [
         pltpu.make_async_copy(src, dst, io_sem.at[i])
         for i, (src, dst) in enumerate((
@@ -113,17 +137,27 @@
         for i, (src, dst) in enumerate(((wg_hbm, wg), (wu_hbm, wu), (wd_hbm, wd)))
     ]
     partner, across_mid = flipped(ep, 1), flipped(ep, 3)
+
+    @pl.when(is_end)
+    def _():
+        pl.semaphore_wait(barrier, near - 1)
+
+    @pl.when(jnp.logical_and(is_end, jnp.logical_not(is_first)))
+    def _():
+        for j in range(tp_count):
+            pl.semaphore_signal(ready, inc=1, device_id=at(partner, j), device_id_type=MESH)
+
     planes = [ep, partner]
     dense = [
-        remote(normed.at[c], rblock.at[0, c], dense_s, dense_r.at[0, c], at(across_mid, 0))
+        remote(normed.at[c], rblock.at[0, c], dense_s, dense_r.at[0, slot(DENSE_BY, c)], at(across_mid, 0))
         for c in range(PIECES)
     ]
     forward = [
-        remote(eblock.at[c], rblock.at[1, c], fwd_s, dense_r.at[1, c], at(across_mid, 0))
+        remote(eblock.at[c], rblock.at[1, c], fwd_s, dense_r.at[1, slot(DENSE_BY, c)], at(across_mid, 0))
         for c in range(PIECES)
     ]
     edense = [
-        remote(normed.at[c], eblock.at[c], dense_s, edense_r.at[c], at(partner, 0))
+        remote(normed.at[c], eblock.at[c], dense_s, edense_r.at[slot(EDENSE_BY, c)], at(partner, 0))
         for c in range(PIECES)
     ]
     far_meta = pl.ds(0, 2 * near)
@@ -133,7 +167,7 @@
                           at(across_mid, 0))
     emeta_copy = remote(meta, emeta, meta_s.at[0], emeta_r.at[0], at(partner, 0))
     near_out = [
-        remote(nsend.at[g], nrecv.at[g], near_s, near_r.at[g // tp_count],
+        remote(nsend.at[g], nrecv.at[g], near_s, near_r.at[max(0, 2 * g // tp_count - 1)],
                at(planes[g // tp_count], g % tp_count))
         for g in range(near)
     ]
@@ -155,19 +189,25 @@
                at(planes[g // tp_count], g % tp_count))
         for g in range(near)
     ]
-    far_out, far_ret, final = {}, {}, {}
+    far_out, far_ret, to_hop, from_hop, final = {}, {}, {}, {}, {}
     for v in range(2):
         for c in range(PIECES):
             for i in range(near):
                 far_out[v, c, i] = remote(
                     fsend.at[v, c, i], frecv.at[v, c, i % tp_count], far_s,
-                    far_r.at[v, c], at(planes[i // tp_count], i % tp_count))
+                    far_r.at[v, slot(FAR_BY, c)], at(planes[i // tp_count], i % tp_count))
             for j in range(tp_count):
                 place = place_of_me + j
                 far_ret[v, c, j] = remote(
-                    fres.at[v, c, j], rback.at[v, c, place], fret_s, fret_r.at[v, c],
+                    fres.at[v, c, j], rback.at[v, c, place], fret_s, fret_r.at[v, slot(BACK_BY, c)],
                     at(own_relay, j))
-            final[v, c] = remote(rsend.at[v, c], farback.at[c], final_s, final_r.at[c],
+            if v == 0 and c >= DIRECT:
+                for j in range(side, tp_count):
+                    to_hop[c, j] = remote(fres.at[v, c, j], hop.at[c, j - side], fret_s,
+                                          hop_r.at[slot(HOP_BY, c)], at(ep, j))
+                from_hop[c] = remote(hop.at[c], rback.at[v, c, pl.ds(tp_count + side, side)],
+                                     hop_s, fret_r.at[v, slot(BACK_BY, c)], at(own_relay, 0))
+            final[v, c] = remote(rsend.at[v, c], farback.at[c], final_s, final_r.at[slot(FINAL_BY, c)],
                                  at(flipped(ep, 3 - v), 0))
 
     def drain(ref, sem):
@@ -206,6 +246,19 @@
     for c in range(PIECES):
         normed[c] = rows_normed[:, c * part_w:(c + 1) * part_w]
 
+    @pl.when(is_boundary)
+    def _():
+        pl.semaphore_wait(barrier, tp_count + jnp.where(is_first, tp_count, 0))
+        meta_copy.start()
+        for c in range(PIECES):
+            dense[c].start()
+
+    @pl.when(is_end)
+    def _():
+        emeta_copy.start()
+        for c in range(PIECES):
+            edense[c].start()
+
     def pick_of(rank):
         count = rank.shape[0]
         slot = lax.broadcasted_iota(jnp.int32, (count, cap, rows), 1).astype(jnp.float32)
@@ -219,28 +272,13 @@
         high = share.astype(jnp.bfloat16)
         return pick, high, (share - high.astype(jnp.float32)).astype(jnp.bfloat16)
 
-    pl.semaphore_wait(barrier, near + boundary)
-
-    @pl.when(is_boundary)
-    def _():
-        meta_copy.start()
-        for c in range(PIECES):
-            dense[c].start()
-
-    @pl.when(is_end)
-    def _():
-        emeta_copy.start()
-        for c in range(PIECES):
-            edense[c].start()
-
     pick, high, low = onehots(rank[:near], weight[:near])
-    share_hi[...] = high
-    share_lo[...] = low
 
     def dot(a, b):
         return jnp.dot(a, b, preferred_element_type=jnp.float32)
 
     half = tp_count * cap
+    crossing = [*range(side, tp_count), *range(side - 1, -1, -1)]
 
     def pack_near(p):
         packed = dot(pick[p * half:(p + 1) * half], rows_normed)
@@ -250,7 +288,11 @@
                 nsend[p * tp_count + j] = packed[j]
             else:
                 nrecv[0] = packed[0]
-        send_near(range(2) if p else range(1, tp_count), p)
+
+    pack_near(1)
+
+    share_hi[...] = high
+    share_lo[...] = low
 
     def send_near(js, p=1):
         for j in js:
@@ -259,24 +301,28 @@
     def hidden_of(gate_act, up_act):
         return (gate_act / (1.0 + jnp.exp(-gate_act)) * up_act).astype(jnp.bfloat16)
 
-    def expert_near(p, first):
-        base = p * tp_count
-        drain(nrecv.at[pl.ds(base + first, tp_count - first)], near_r.at[p])
-        block = nrecv[base:base + tp_count].reshape(half, width)
+    def near_part(base, first, count, sem):
+        drain(nrecv.at[pl.ds(base + first, count - first)], near_r.at[sem])
+        block = nrecv[base:base + count].reshape(count * cap, width)
         hidden = hidden_of(dot(block, wg[...]), dot(block, wu[...]))
-        result = dot(hidden, wd[...]).astype(jnp.bfloat16).reshape(tp_count, cap, width)
-        for j in range(tp_count):
-            if p or j:
+        result = dot(hidden, wd[...]).astype(jnp.bfloat16).reshape(count, cap, width)
+        for j in range(count):
+            if base or j:
                 nres[base + j] = result[j]
             else:
                 nback[0] = result[0]
 
+    def expert_near(p, first):
+        near_part(p * tp_count, first, tp_count, p)
+
     def return_near(gs):
         for g in gs:
             near_ret[g].start()
 
     def forward_end(c):
-        edense[c].wait_recv()
+        g, lo, count = span(EDENSE_BY, c)
+        if c == lo:
+            drain(eblock.at[pl.ds(lo, count)], edense_r.at[g])
         forward[c].start()
 
     def end_meta():
@@ -293,12 +339,9 @@
         for j in range(1, side):
             eout[j].start()
 
-    def pack_lend():
-        packed = dot(pick[half + side * cap:], rows_normed)
-        packed = packed.astype(jnp.bfloat16).reshape(tp_count - side, cap, width)
-        for k in range(side):
-            nsend[tp_count + side + k] = packed[k]
-            lend[k].start()
+    def send_lend():
+        for copy in lend:
+            copy.start()
 
     def send_lent():
         drain(esend, lend_r)
@@ -318,17 +361,20 @@
         rshare_lo[v] = rl
 
     def relay_out(v, c):
-        remote(normed.at[c], rblock.at[v, c], dense_s, dense_r.at[v, c],
-               at(across_mid, 0)).wait_recv()
+        g, lo, count = span(DENSE_BY, c)
+        if c == lo:
+            drain(rblock.at[v, pl.ds(lo, count)], dense_r.at[v, g])
         packed = dot(rpick[v], rblock[v, c]).astype(jnp.bfloat16).reshape(near, cap, part_w)
         frecv[v, c, 0] = packed[0]
         for i in range(1, near):
             fsend[v, c, i] = packed[i]
-        for i in list(range(tp_count, near)) + list(range(1, tp_count)):
+        for i in list(range(tp_count + side, near)) + list(range(tp_count, tp_count + side)) + crossing[:-1]:
             far_out[v, c, i].start()
 
     def far_in(v, c, first):
-        drain(frecv.at[v, c, pl.ds(first, tp_count - first)], far_r.at[v, c])
+        g, lo, count = span(FAR_BY, c)
+        if c == lo:
+            drain(frecv.at[v, pl.ds(lo, count), pl.ds(first, tp_count - first)], far_r.at[v, g])
         block = frecv[v, c].reshape(half, part_w)
         more_gate = dot(block, wg[c * part_w:(c + 1) * part_w])
         more_up = dot(block, wu[c * part_w:(c + 1) * part_w])
@@ -346,8 +392,17 @@
                     rback[v, c, 0] = part[0]
                 for j in range(at_relay, tp_count):
                     fres[v, c, j] = part[j]
-                for j in range(at_relay, tp_count):
-                    far_ret[v, c, j].start()
+                for j in crossing[:tp_count - at_relay]:
+                    if not at_relay and (c, j) in to_hop and v == 0:
+                        to_hop[c, j].start()
+                    else:
+                        far_ret[v, c, j].start()
+
+    def hop_on(c):
+        g, lo, count = span(HOP_BY, c)
+        if c == lo:
+            drain(hop.at[pl.ds(lo, count)], hop_r.at[g])
+        from_hop[c].start()
 
     def combine(high, low, block):
         total = None
@@ -359,7 +414,9 @@
         return total
 
     def relay_back(v, c):
-        drain(rback.at[v, c, pl.ds(1, near - 1)], fret_r.at[v, c])
+        g, lo, count = span(BACK_BY, c)
+        if c == lo:
+            drain(rback.at[v, pl.ds(lo, count), pl.ds(1, near - 1)], fret_r.at[v, g])
         block = rback[v, c].reshape(near * cap, part_w)
         rsend[v, c] = combine(rshare_hi[v], rshare_lo[v], block).astype(jnp.bfloat16)
         final[v, c].start()
@@ -369,12 +426,19 @@
         acc[...] = combine(share_hi[...], share_lo[...], nback[...].reshape(near * cap, width))
 
     def finish(c):
-        final[0, c].wait_recv()
+        g, lo, count = span(FINAL_BY, c)
+        if c == lo:
+            drain(farback.at[pl.ds(lo, count)], final_r.at[g])
         part = acc[:, c * part_w:(c + 1) * part_w] + farback[c].astype(jnp.float32)
         out_ref[:, c * part_w:(c + 1) * part_w] = part.astype(out_ref.dtype)
 
     others = range(1, tp_count)
     second = range(tp_count, near)
+
+    def ends_here():
+        @pl.when(jnp.logical_not(is_first))
+        def _():
+            pl.semaphore_wait(ready, tp_count)
 
     def weights_here():
         for load in loads:
@@ -382,8 +446,18 @@
 
     @pl.when(is_boundary)
     def _():
+        @pl.when(is_first)
+        def _():
+            send_near(range(AHEAD))
+
         pack_near(0)
-        pack_near(1)
+        send_near(range(1, tp_count), 0)
+        ends_here()
+
+        @pl.when(jnp.logical_not(is_first))
+        def _():
+            send_near(range(AHEAD))
+
         relay_meta(0)
         last = PIECES - 1
         ahead = PIECES // 2
@@ -400,7 +474,7 @@
             relay_out(0, c)
             forward_end(c - 1)
         forward_end(last)
-        send_near(range(2, tp_count))
+        send_near(range(AHEAD, tp_count))
         pack_end()
         relay_meta(1)
         for c in range(PIECES // 2):
@@ -409,42 +483,72 @@
         for c in range(PIECES // 2, PIECES):
             far_in(0, c, 1)
         far_result(0, 1)
-        for c in range(1, PIECES - 1):
+        relay_out(1, 1)
+        expert_near(1, 1)
+        for c in range(2, PIECES - 3):
             relay_out(1, c)
         relay_back(0, 0)
+        relay_out(1, last - 2)
+        relay_back(0, 1)
+        relay_out(1, last - 1)
         relay_out(1, last)
-        relay_back(0, 1)
-        expert_near(1, 1)
-        return_near(second)
+
+        @pl.when(tp < side)
+        def _():
+            return_near(second)
+
+        @pl.when(tp >= side)
+        def _():
+            return_near(second[::-1])
+
         relay_back(0, 2)
         relay_back(0, 3)
-        for c in range(4, PIECES):
+        for c in range(4, 6):
             far_in(1, 2 * c - 8, 1)
             far_in(1, 2 * c - 7, 1)
             relay_back(0, c)
+        for c in range(4, PIECES):
+            far_in(1, c, 1)
         far_result(1, 1)
+        relay_back(0, last - 1)
+
+        @pl.when(jnp.logical_not(holds_back))
+        def _():
+            relay_back(0, last)
+
         for c in range(PIECES):
             relay_back(1, c)
+
+        @pl.when(holds_back)
+        def _():
+            relay_back(0, last)
+
         combine_near()
         for c in range(PIECES):
             finish(c)
 
     @pl.when(is_end)
     def _():
+        send_lend()
         pack_near(0)
-        pack_lend()
+        send_near(range(1, tp_count), 0)
+        send_lent()
         weights_here()
-        expert_near(0, 1)
-        return_near(others)
-        send_lent()
+        near_part(tp_count, 0, side, 1)
+        return_near(list(second)[:EARLY])
         for c in range(PIECES):
             far_in(0, c, 0)
         far_result(0, 0)
-        expert_near(1, 0)
-        return_near(list(second)[:EARLY])
+        for c in range(DIRECT, PIECES):
+            if c == DIRECT + 2:
+                expert_near(0, 1)
+            if c == DIRECT + 4:
+                near_part(tp_count + side, 0, tp_count - side, 2)
+            hop_on(c)
         for c in range(PIECES):
             far_in(1, c, 0)
         far_result(1, 0)
+        return_near(others)
         return_near(list(second)[EARLY:])
         combine_near()
         for c in range(PIECES):
@@ -459,6 +563,7 @@
         drain(nsend.at[pl.ds(1, tp_count + side - 1)], near_s)
         drain(esend, eout_s)
         drain(fres, fret_s)
+        drain(hop.at[pl.ds(DIRECT, PIECES - DIRECT)], hop_s)
 
     @pl.when(is_boundary)
     def _():
@@ -505,6 +610,7 @@
             *[b16(near, cap, width)] * 4,
             b16(PIECES, rows, part_w), f32(3 * near, rows),
             b16(tp_count // 2 * cap, rows), b16(tp_count // 2, cap, width),
+            b16(PIECES, tp_count // 2, cap, part_w),
             b16(2, PIECES, rows, part_w), f32(2, 2 * near, rows),
             *[b16(2, near * cap, rows)] * 3,
             b16(2, PIECES, near, cap, part_w),
@@ -514,9 +620,11 @@
             b16(2, PIECES, rows, part_w), b16(PIECES, rows, part_w),
             b16(width, hidden), b16(width, hidden), b16(hidden, width),
             f32(rows, width), f32(tp_count * cap, hidden), f32(tp_count * cap, hidden),
-            sems(3), one, one, sems(PIECES), sems(2, PIECES),
-            sems(2), sems(1), sems(2), one, sems(2), one, one, one, one,
-            one, sems(2, PIECES), one, sems(2, PIECES), one, sems(PIECES),
+            sems(3), pltpu.SemaphoreType.REGULAR, one, one,
+            sems(len(EDENSE_BY) - 1), sems(2, len(DENSE_BY) - 1),
+            sems(2), sems(1), sems(2), one, sems(3), one, one, one, one,
+            one, sems(2, len(FAR_BY) - 1), one, sems(2, len(BACK_BY) - 1),
+            one, sems(len(HOP_BY) - 1), one, sems(len(FINAL_BY) - 1),
         ],
         compiler_params=pltpu.CompilerParams(
             collective_id=0, has_side_effects=True, vmem_limit_bytes=32 * 1024 * 1024

time: 56.9 us -> 54.4 us (0.956)
  Pallas kernels: 55.9 us -> 53.5 us
    pallas_call x1, Pallas kernels: 55.9 us -> 53.5 us  [fused(): pl.pallas_call(functools.partial(kernel, ep_count, tp_count, cap), out_sh...]
where the time goes in v3:
time: 54.4 us; the launch traced here: 54.3 us
  Pallas kernels  53.5 us (98%)
  local copies, waits for them, and re-layouts  0.8 us (1%)
    pallas_call x1, Pallas kernels, fused(): pl.pallas_call(functools.partial(kernel, ep_count, tp_count, cap), out_sh...  53.5 us

profile of v3, /device:TPU:0, one launch (start us, length us, event | category | flops | bytes accessed | tf_op | source)
XLA Modules:
  0.0 54.3 jit_solution(9304250867466396774)
XLA Ops:
  0.0 53.5 %shard_map.73 = bf16[128,2048]{1,0:T(8,128)(2,1)S(1)} custom-call(bf16[128,2048]{1,0:T(8,128)(2,1)} %x_hbm.1, f32[1,2048]{1,0:T(1,128)} %bitcast.3, s32[2,128]{1,0:T(2,128)} %bitcast.4, f32[2,128]{1,0:T(2,128)} %bitcast.5, bf16[1,2048,512]{2,1,0:T(8,128)(2,1)} %wg_hbm.1, bf16[1,2048,512]{2,1,0:T(8,128)(2,1)} %wu_hbm.1, bf16[1,512,2048]{2,1,0:T(8,128)(2,1)} %wd_hbm.1), custom_call_target="tpu_custom_call" | custom-call | tf_op jit(solution)/shard_map/pallas_call | solution.py:600
  53.5 0.8 %copy.9 = bf16[128,2048]{1,0:T(8,128)(2,1)} copy(bf16[128,2048]{1,0:T(8,128)(2,1)S(1)} %shard_map.73) | data formatting | bytes 1048576

commit v4 on v3

--- a/solution.py
+++ b/solution.py
@@ -54,14 +54,14 @@
 PIECES = 8
 EARLY = 1
 AHEAD = 3
-DIRECT = 2
+DIRECT = 3
 GROUPS = ((0, 1), (1, 3), (3, 8))
-DENSE_BY = (0, 2, 4, 6, 7, 8)
-EDENSE_BY = (0, 2, 4, 6, 8)
+DENSE_BY = ((0, 2, 3, 4, 5, 6, 7, 8), (0, 1, 2, 3, 4, 5, 6, 7, 8))
+EDENSE_BY = (0, 4, 6, 8)
 FAR_BY = (0, 4, 6, 7, 8)
-BACK_BY = (0, 1, 2, 3, 4, 5, 6, 7, 8)
+BACK_BY = ((0, 1, 2, 3, 4, 6, 8), (0, 1, 2, 3, 5, 7, 8))
 HOP_BY = (DIRECT, 4, 6, 8)
-FINAL_BY = (0, 6, 7, 8)
+FINAL_BY = (0, 7, 8)
 
 
 def span(edges, c):
@@ -149,11 +149,11 @@
 
     planes = [ep, partner]
     dense = [
-        remote(normed.at[c], rblock.at[0, c], dense_s, dense_r.at[0, slot(DENSE_BY, c)], at(across_mid, 0))
+        remote(normed.at[c], rblock.at[0, c], dense_s, dense_r.at[slot(DENSE_BY[0], c)], at(across_mid, 0))
         for c in range(PIECES)
     ]
     forward = [
-        remote(eblock.at[c], rblock.at[1, c], fwd_s, dense_r.at[1, slot(DENSE_BY, c)], at(across_mid, 0))
+        remote(eblock.at[c], rblock.at[1, c], fwd_s, dense_r.at[len(DENSE_BY[0]) - 1 + slot(DENSE_BY[1], c)], at(across_mid, 0))
         for c in range(PIECES)
     ]
     edense = [
@@ -199,19 +199,43 @@
             for j in range(tp_count):
                 place = place_of_me + j
                 far_ret[v, c, j] = remote(
-                    fres.at[v, c, j], rback.at[v, c, place], fret_s, fret_r.at[v, slot(BACK_BY, c)],
+                    fres.at[v, c, j], rback.at[v, c, place], fret_s, fret_r.at[v, slot(BACK_BY[v], c)],
                     at(own_relay, j))
             if v == 0 and c >= DIRECT:
                 for j in range(side, tp_count):
                     to_hop[c, j] = remote(fres.at[v, c, j], hop.at[c, j - side], fret_s,
                                           hop_r.at[slot(HOP_BY, c)], at(ep, j))
                 from_hop[c] = remote(hop.at[c], rback.at[v, c, pl.ds(tp_count + side, side)],
-                                     hop_s, fret_r.at[v, slot(BACK_BY, c)], at(own_relay, 0))
+                                     hop_s, fret_r.at[v, slot(BACK_BY[v], c)], at(own_relay, 0))
             final[v, c] = remote(rsend.at[v, c], farback.at[c], final_s, final_r.at[slot(FINAL_BY, c)],
                                  at(flipped(ep, 3 - v), 0))
 
     def drain(ref, sem):
         pltpu.make_async_copy(ref, ref, sem).wait()
+
+    for fetch in fetches[:2]:
+        fetch.wait()
+    for load in loads:
+        load.start()
+    values = x_ref[...].astype(jnp.float32)
+    rows_normed = (
+        values
+        * lax.rsqrt(jnp.mean(values * values, axis=-1, keepdims=True) + 1e-06)
+        * gain_ref[...]
+    ).astype(jnp.bfloat16)
+    for c in range(PIECES):
+        normed[c] = rows_normed[:, c * part_w:(c + 1) * part_w]
+
+    @pl.when(is_boundary)
+    def _():
+        pl.semaphore_wait(barrier, tp_count + jnp.where(is_first, tp_count, 0))
+        for c in range(2):
+            dense[c].start()
+
+    @pl.when(is_end)
+    def _():
+        for c in range(2):
+            edense[c].start()
 
     down = lax.broadcasted_iota(jnp.int32, (rows, rows), 0)
     across = lax.broadcasted_iota(jnp.int32, (rows, rows), 1)
@@ -233,30 +257,16 @@
     meta[near:2 * near] = weight[near:]
     meta[2 * near:] = rank[:near]
 
-    for fetch in fetches[:2]:
-        fetch.wait()
-    for load in loads:
-        load.start()
-    values = x_ref[...].astype(jnp.float32)
-    rows_normed = (
-        values
-        * lax.rsqrt(jnp.mean(values * values, axis=-1, keepdims=True) + 1e-06)
-        * gain_ref[...]
-    ).astype(jnp.bfloat16)
-    for c in range(PIECES):
-        normed[c] = rows_normed[:, c * part_w:(c + 1) * part_w]
-
     @pl.when(is_boundary)
     def _():
-        pl.semaphore_wait(barrier, tp_count + jnp.where(is_first, tp_count, 0))
         meta_copy.start()
-        for c in range(PIECES):
+        for c in range(2, PIECES):
             dense[c].start()
 
     @pl.when(is_end)
     def _():
         emeta_copy.start()
-        for c in range(PIECES):
+        for c in range(2, PIECES):
             edense[c].start()
 
     def pick_of(rank):
@@ -361,9 +371,9 @@
         rshare_lo[v] = rl
 
     def relay_out(v, c):
-        g, lo, count = span(DENSE_BY, c)
+        g, lo, count = span(DENSE_BY[v], c)
         if c == lo:
-            drain(rblock.at[v, pl.ds(lo, count)], dense_r.at[v, g])
+            drain(rblock.at[v, pl.ds(lo, count)], dense_r.at[v * (len(DENSE_BY[0]) - 1) + g])
         packed = dot(rpick[v], rblock[v, c]).astype(jnp.bfloat16).reshape(near, cap, part_w)
         frecv[v, c, 0] = packed[0]
         for i in range(1, near):
@@ -395,8 +405,12 @@
                 for j in crossing[:tp_count - at_relay]:
                     if not at_relay and (c, j) in to_hop and v == 0:
                         to_hop[c, j].start()
-                    else:
+                    elif at_relay or v or c <= DIRECT:
                         far_ret[v, c, j].start()
+
+    def late_return(c):
+        for j in crossing[side:]:
+            far_ret[0, c, j].start()
 
     def hop_on(c):
         g, lo, count = span(HOP_BY, c)
@@ -414,7 +428,7 @@
         return total
 
     def relay_back(v, c):
-        g, lo, count = span(BACK_BY, c)
+        g, lo, count = span(BACK_BY[v], c)
         if c == lo:
             drain(rback.at[v, pl.ds(lo, count), pl.ds(1, near - 1)], fret_r.at[v, g])
         block = rback[v, c].reshape(near * cap, part_w)
@@ -474,24 +488,33 @@
             relay_out(0, c)
             forward_end(c - 1)
         forward_end(last)
-        send_near(range(AHEAD, tp_count))
+
+        @pl.when(is_first)
+        def _():
+            send_near(range(AHEAD, tp_count))
+
+        relay_meta(1)
         pack_end()
-        relay_meta(1)
+        relay_out(1, 0)
         for c in range(PIECES // 2):
             far_in(0, c, 1)
-        relay_out(1, 0)
+        relay_out(1, 1)
         for c in range(PIECES // 2, PIECES):
             far_in(0, c, 1)
         far_result(0, 1)
-        relay_out(1, 1)
+        relay_out(1, 2)
+        relay_out(1, 3)
         expert_near(1, 1)
-        for c in range(2, PIECES - 3):
-            relay_out(1, c)
+        relay_out(1, 4)
+        relay_out(1, 5)
         relay_back(0, 0)
-        relay_out(1, last - 2)
+        relay_out(1, 6)
         relay_back(0, 1)
-        relay_out(1, last - 1)
-        relay_out(1, last)
+        relay_out(1, 7)
+
+        @pl.when(jnp.logical_not(is_first))
+        def _():
+            send_near(range(AHEAD, tp_count))
 
         @pl.when(tp < side)
         def _():
@@ -503,13 +526,13 @@
 
         relay_back(0, 2)
         relay_back(0, 3)
-        for c in range(4, 6):
-            far_in(1, 2 * c - 8, 1)
-            far_in(1, 2 * c - 7, 1)
-            relay_back(0, c)
+        for c in range(4):
+            far_in(1, c, 1)
+        relay_back(0, 4)
         for c in range(4, PIECES):
             far_in(1, c, 1)
         far_result(1, 1)
+        relay_back(0, 5)
         relay_back(0, last - 1)
 
         @pl.when(jnp.logical_not(holds_back))
@@ -539,17 +562,27 @@
         for c in range(PIECES):
             far_in(0, c, 0)
         far_result(0, 0)
-        for c in range(DIRECT, PIECES):
-            if c == DIRECT + 2:
-                expert_near(0, 1)
-            if c == DIRECT + 4:
-                near_part(tp_count + side, 0, tp_count - side, 2)
-            hop_on(c)
-        for c in range(PIECES):
+        hop_on(3)
+        late_return(4)
+        late_return(5)
+        expert_near(0, 1)
+        for c in range(4):
             far_in(1, c, 0)
+        hop_on(4)
+        hop_on(5)
+        late_return(6)
+        late_return(7)
+        far_in(1, 4, 0)
+        far_in(1, 5, 0)
+        hop_on(6)
+        hop_on(7)
+        far_in(1, 6, 0)
+        far_in(1, 7, 0)
         far_result(1, 0)
         return_near(others)
-        return_near(list(second)[EARLY:])
+        return_near(list(second)[EARLY:side])
+        near_part(tp_count + side, 0, tp_count - side, 2)
+        return_near(list(second)[side:])
         combine_near()
         for c in range(PIECES):
             finish(c)
@@ -621,9 +654,9 @@
             b16(width, hidden), b16(width, hidden), b16(hidden, width),
             f32(rows, width), f32(tp_count * cap, hidden), f32(tp_count * cap, hidden),
             sems(3), pltpu.SemaphoreType.REGULAR, one, one,
-            sems(len(EDENSE_BY) - 1), sems(2, len(DENSE_BY) - 1),
+            sems(len(EDENSE_BY) - 1), sems(sum(map(len, DENSE_BY)) - 2),
             sems(2), sems(1), sems(2), one, sems(3), one, one, one, one,
-            one, sems(2, len(FAR_BY) - 1), one, sems(2, len(BACK_BY) - 1),
+            one, sems(2, len(FAR_BY) - 1), one, sems(2, len(BACK_BY[0]) - 1),
             one, sems(len(HOP_BY) - 1), one, sems(len(FINAL_BY) - 1),
         ],
         compiler_params=pltpu.CompilerParams(

time: 54.4 us -> 53.1 us (0.976)
  Pallas kernels: 53.5 us -> 52.2 us
    pallas_call x1, Pallas kernels: 53.5 us -> 52.2 us  [fused(): pl.pallas_call(functools.partial(kernel, ep_count, tp_count, cap), out_sh...]
where the time goes in v4:
time: 53.1 us; the launch traced here: 53 us
  Pallas kernels  52.2 us (98%)
  local copies, waits for them, and re-layouts  0.8 us (2%)
    pallas_call x1, Pallas kernels, fused(): pl.pallas_call(functools.partial(kernel, ep_count, tp_count, cap), out_sh...  52.2 us

profile of v4, /device:TPU:0, one launch (start us, length us, event | category | flops | bytes accessed | tf_op | source)
XLA Modules:
  0.0 53.0 jit_solution(9742598736305676366)
XLA Ops:
  0.0 52.2 %shard_map.73 = bf16[128,2048]{1,0:T(8,128)(2,1)S(1)} custom-call(bf16[128,2048]{1,0:T(8,128)(2,1)} %x_hbm.1, f32[1,2048]{1,0:T(1,128)} %bitcast.3, s32[2,128]{1,0:T(2,128)} %bitcast.4, f32[2,128]{1,0:T(2,128)} %bitcast.5, bf16[1,2048,512]{2,1,0:T(8,128)(2,1)} %wg_hbm.1, bf16[1,2048,512]{2,1,0:T(8,128)(2,1)} %wu_hbm.1, bf16[1,512,2048]{2,1,0:T(8,128)(2,1)} %wd_hbm.1), custom_call_target="tpu_custom_call" | custom-call | tf_op jit(solution)/shard_map/pallas_call | solution.py:633
  52.2 0.8 %copy.9 = bf16[128,2048]{1,0:T(8,128)(2,1)} copy(bf16[128,2048]{1,0:T(8,128)(2,1)S(1)} %shard_map.73) | data formatting | bytes 1048576

commit v5 on v4

--- a/solution.py
+++ b/solution.py
@@ -59,9 +59,10 @@
 DENSE_BY = ((0, 2, 3, 4, 5, 6, 7, 8), (0, 1, 2, 3, 4, 5, 6, 7, 8))
 EDENSE_BY = (0, 4, 6, 8)
 FAR_BY = (0, 4, 6, 7, 8)
-BACK_BY = ((0, 1, 2, 3, 4, 6, 8), (0, 1, 2, 3, 5, 7, 8))
+BACK_BY = ((0, 1, 2, 3, 4, 5, 6, 8), (0, 1, 2, 3, 4, 5, 6, 7, 8))
 HOP_BY = (DIRECT, 4, 6, 8)
 FINAL_BY = (0, 7, 8)
+WAVE_AT = (0, len(DENSE_BY[0]) - 1)
 
 
 def span(edges, c):
@@ -82,7 +83,7 @@
     rblock, rmeta, rpick, rshare_hi, rshare_lo, fsend, frecv, fres, rback, rsend, farback,
     wg, wu, wd, acc, gate_acc, up_acc,
     w_sem, ready, dense_s, fwd_s, edense_r, dense_r, meta_s, emeta_r, meta_r, near_s, near_r,
-    eout_s, lend_r, nret_s, nret_r, far_s, far_r, fret_s, fret_r, hop_s, hop_r, final_s, final_r,
+    eout_s, far_s, far_r,
 ):
     ep, tp, grp = lax.axis_index("ep"), lax.axis_index("tp"), lax.axis_index("grp")
     rows, width = x_ref.shape
@@ -96,7 +97,8 @@
     own_relay = 1 + ep // 2
     is_boundary, is_end = boundary == 1, boundary == 0
     is_first = ep < ep_count // 2
-    holds_back = jnp.logical_and(ep == ep_count // 2, tp % 2 == 0)
+    is_late = tp % 2 == 1
+    holds_back = ep == ep_count // 2
 
     def at(plane, j):
         return (grp, plane, flipped(tp, j))
@@ -153,7 +155,7 @@
         for c in range(PIECES)
     ]
     forward = [
-        remote(eblock.at[c], rblock.at[1, c], fwd_s, dense_r.at[len(DENSE_BY[0]) - 1 + slot(DENSE_BY[1], c)], at(across_mid, 0))
+        remote(eblock.at[c], rblock.at[1, c], fwd_s, dense_r.at[WAVE_AT[1] + slot(DENSE_BY[1], c)], at(across_mid, 0))
         for c in range(PIECES)
     ]
     edense = [
@@ -161,11 +163,11 @@
         for c in range(PIECES)
     ]
     far_meta = pl.ds(0, 2 * near)
-    meta_copy = remote(meta.at[far_meta], rmeta.at[0], meta_s.at[0], meta_r.at[0],
+    meta_copy = remote(meta.at[far_meta], rmeta.at[0], meta_s, meta_r.at[0],
                        at(across_mid, 0))
-    meta_forward = remote(emeta.at[far_meta], rmeta.at[1], meta_s.at[1], meta_r.at[1],
+    meta_forward = remote(emeta.at[far_meta], rmeta.at[1], meta_s, meta_r.at[1],
                           at(across_mid, 0))
-    emeta_copy = remote(meta, emeta, meta_s.at[0], emeta_r.at[0], at(partner, 0))
+    emeta_copy = remote(meta, emeta, meta_s, emeta_r.at[0], at(partner, 0))
     near_out = [
         remote(nsend.at[g], nrecv.at[g], near_s, near_r.at[max(0, 2 * g // tp_count - 1)],
                at(planes[g // tp_count], g % tp_count))
@@ -177,7 +179,7 @@
         for j in range(side)
     ]
     lend = [
-        remote(nsend.at[tp_count + side + k], esend.at[k], near_s, lend_r, at(ep, side))
+        remote(nsend.at[tp_count + side + k], esend.at[k], near_s, dense_r.at[len(HOP_BY)], at(ep, side))
         for k in range(side)
     ]
     pass_on = [
@@ -185,7 +187,7 @@
         for k in range(side)
     ]
     near_ret = [
-        remote(nres.at[g], nback.at[g], nret_s, nret_r,
+        remote(nres.at[g], nback.at[g], w_sem.at[0], io_sem.at[2 + g // tp_count],
                at(planes[g // tp_count], g % tp_count))
         for g in range(near)
     ]
@@ -199,15 +201,15 @@
             for j in range(tp_count):
                 place = place_of_me + j
                 far_ret[v, c, j] = remote(
-                    fres.at[v, c, j], rback.at[v, c, place], fret_s, fret_r.at[v, slot(BACK_BY[v], c)],
+                    fres.at[v, c, j], rback.at[v, c, place], w_sem.at[1], dense_r.at[WAVE_AT[v] + slot(BACK_BY[v], c)],
                     at(own_relay, j))
             if v == 0 and c >= DIRECT:
                 for j in range(side, tp_count):
-                    to_hop[c, j] = remote(fres.at[v, c, j], hop.at[c, j - side], fret_s,
-                                          hop_r.at[slot(HOP_BY, c)], at(ep, j))
+                    to_hop[c, j] = remote(fres.at[v, c, j], hop.at[c, j - side], w_sem.at[1],
+                                          dense_r.at[slot(HOP_BY, c)], at(ep, j))
                 from_hop[c] = remote(hop.at[c], rback.at[v, c, pl.ds(tp_count + side, side)],
-                                     hop_s, fret_r.at[v, slot(BACK_BY[v], c)], at(own_relay, 0))
-            final[v, c] = remote(rsend.at[v, c], farback.at[c], final_s, final_r.at[slot(FINAL_BY, c)],
+                                     fwd_s, dense_r.at[WAVE_AT[v] + slot(BACK_BY[v], c)], at(own_relay, 0))
+            final[v, c] = remote(rsend.at[v, c], farback.at[c], w_sem.at[2], io_sem.at[slot(FINAL_BY, c)],
                                  at(flipped(ep, 3 - v), 0))
 
     def drain(ref, sem):
@@ -354,12 +356,12 @@
             copy.start()
 
     def send_lent():
-        drain(esend, lend_r)
+        drain(esend, dense_r.at[len(HOP_BY)])
         for copy in pass_on:
             copy.start()
 
     def relay_meta(v):
-        remote(meta.at[far_meta], rmeta.at[v], meta_s.at[0], meta_r.at[v],
+        remote(meta.at[far_meta], rmeta.at[v], meta_s, meta_r.at[v],
                at(across_mid, 0)).wait_recv()
         ranks, weights = rmeta[v, 0:near], rmeta[v, near:]
         if v == 0:
@@ -373,7 +375,7 @@
     def relay_out(v, c):
         g, lo, count = span(DENSE_BY[v], c)
         if c == lo:
-            drain(rblock.at[v, pl.ds(lo, count)], dense_r.at[v * (len(DENSE_BY[0]) - 1) + g])
+            drain(rblock.at[v, pl.ds(lo, count)], dense_r.at[WAVE_AT[v] + g])
         packed = dot(rpick[v], rblock[v, c]).astype(jnp.bfloat16).reshape(near, cap, part_w)
         frecv[v, c, 0] = packed[0]
         for i in range(1, near):
@@ -415,7 +417,7 @@
     def hop_on(c):
         g, lo, count = span(HOP_BY, c)
         if c == lo:
-            drain(hop.at[pl.ds(lo, count)], hop_r.at[g])
+            drain(hop.at[pl.ds(lo, count)], dense_r.at[g])
         from_hop[c].start()
 
     def combine(high, low, block):
@@ -430,19 +432,24 @@
     def relay_back(v, c):
         g, lo, count = span(BACK_BY[v], c)
         if c == lo:
-            drain(rback.at[v, pl.ds(lo, count), pl.ds(1, near - 1)], fret_r.at[v, g])
+            drain(rback.at[v, pl.ds(lo, count), pl.ds(1, near - 1)], dense_r.at[WAVE_AT[v] + g])
         block = rback[v, c].reshape(near * cap, part_w)
         rsend[v, c] = combine(rshare_hi[v], rshare_lo[v], block).astype(jnp.bfloat16)
         final[v, c].start()
 
     def combine_near():
-        drain(nback.at[pl.ds(1, near - 1)], nret_r)
-        acc[...] = combine(share_hi[...], share_lo[...], nback[...].reshape(near * cap, width))
+        for p in range(2):
+            lo = p * half
+            first = p * tp_count + 1 - p
+            drain(nback.at[pl.ds(first, tp_count - 1 + p)], io_sem.at[2 + p])
+            block = nback[p * tp_count:(p + 1) * tp_count].reshape(half, width)
+            part = combine(share_hi[lo:lo + half], share_lo[lo:lo + half], block)
+            acc[...] = acc[...] + part if p else part
 
     def finish(c):
         g, lo, count = span(FINAL_BY, c)
         if c == lo:
-            drain(farback.at[pl.ds(lo, count)], final_r.at[g])
+            drain(farback.at[pl.ds(lo, count)], io_sem.at[g])
         part = acc[:, c * part_w:(c + 1) * part_w] + farback[c].astype(jnp.float32)
         out_ref[:, c * part_w:(c + 1) * part_w] = part.astype(out_ref.dtype)
 
@@ -470,7 +477,11 @@
 
         @pl.when(jnp.logical_not(is_first))
         def _():
-            send_near(range(AHEAD))
+            send_near(range(AHEAD - 1))
+
+        @pl.when(jnp.logical_not(jnp.logical_or(is_first, is_late)))
+        def _():
+            send_near([AHEAD - 1])
 
         relay_meta(0)
         last = PIECES - 1
@@ -492,6 +503,10 @@
         @pl.when(is_first)
         def _():
             send_near(range(AHEAD, tp_count))
+
+        @pl.when(jnp.logical_and(jnp.logical_not(is_first), is_late))
+        def _():
+            send_near([AHEAD - 1])
 
         relay_meta(1)
         pack_end()
@@ -588,26 +603,25 @@
             finish(c)
 
     drain(normed, dense_s)
-    drain(nres.at[pl.ds(1, near - 1)], nret_s)
+    drain(nres.at[pl.ds(1, near - 1)], w_sem.at[0])
 
     @pl.when(is_end)
     def _():
-        drain(meta, meta_s.at[0])
+        drain(meta, meta_s)
         drain(nsend.at[pl.ds(1, tp_count + side - 1)], near_s)
         drain(esend, eout_s)
-        drain(fres, fret_s)
-        drain(hop.at[pl.ds(DIRECT, PIECES - DIRECT)], hop_s)
+        drain(fres, w_sem.at[1])
+        drain(hop.at[pl.ds(DIRECT, PIECES - DIRECT)], fwd_s)
 
     @pl.when(is_boundary)
     def _():
-        drain(meta.at[far_meta], meta_s.at[0])
-        drain(meta.at[far_meta], meta_s.at[1])
+        drain(rmeta, meta_s)
         drain(eblock, fwd_s)
         drain(nsend.at[pl.ds(1, near - 1)], near_s)
         drain(esend.at[pl.ds(1, side - 1)], eout_s)
-        drain(fres.at[:, :, pl.ds(1, tp_count - 1)], fret_s)
+        drain(fres.at[:, :, pl.ds(1, tp_count - 1)], w_sem.at[1])
         drain(fsend.at[:, :, pl.ds(1, near - 1)], far_s)
-        drain(rsend, final_s)
+        drain(rsend, w_sem.at[2])
 
 
 def fused(ep_count, tp_count, tokens, norm_gain, route_ids, route_weights, w_gate, w_up, w_down):
@@ -655,9 +669,7 @@
             f32(rows, width), f32(tp_count * cap, hidden), f32(tp_count * cap, hidden),
             sems(3), pltpu.SemaphoreType.REGULAR, one, one,
             sems(len(EDENSE_BY) - 1), sems(sum(map(len, DENSE_BY)) - 2),
-            sems(2), sems(1), sems(2), one, sems(3), one, one, one, one,
-            one, sems(2, len(FAR_BY) - 1), one, sems(2, len(BACK_BY[0]) - 1),
-            one, sems(len(HOP_BY) - 1), one, sems(len(FINAL_BY) - 1),
+            one, sems(1), sems(2), one, sems(3), one, one, sems(2, len(FAR_BY) - 1),
         ],
         compiler_params=pltpu.CompilerParams(
             collective_id=0, has_side_effects=True, vmem_limit_bytes=32 * 1024 * 1024

time: 53.1 us -> 52.5 us (0.989)
  Pallas kernels: 52.2 us -> 51.6 us
    pallas_call x1, Pallas kernels: 52.2 us -> 51.6 us  [fused(): pl.pallas_call(functools.partial(kernel, ep_count, tp_count, cap), out_sh...]
where the time goes in v5:
time: 52.5 us; the launch traced here: 52.4 us
  Pallas kernels  51.6 us (98%)
  local copies, waits for them, and re-layouts  0.8 us (2%)
    pallas_call x1, Pallas kernels, fused(): pl.pallas_call(functools.partial(kernel, ep_count, tp_count, cap), out_sh...  51.6 us

profile of v5, /device:TPU:0, one launch (start us, length us, event | category | flops | bytes accessed | tf_op | source)
XLA Modules:
  0.0 52.4 jit_solution(5663199081629621580)
XLA Ops:
  0.0 51.6 %shard_map.73 = bf16[128,2048]{1,0:T(8,128)(2,1)S(1)} custom-call(bf16[128,2048]{1,0:T(8,128)(2,1)} %x_hbm.1, f32[1,2048]{1,0:T(1,128)} %bitcast.3, s32[2,128]{1,0:T(2,128)} %bitcast.4, f32[2,128]{1,0:T(2,128)} %bitcast.5, bf16[1,2048,512]{2,1,0:T(8,128)(2,1)} %wg_hbm.1, bf16[1,2048,512]{2,1,0:T(8,128)(2,1)} %wu_hbm.1, bf16[1,512,2048]{2,1,0:T(8,128)(2,1)} %wd_hbm.1), custom_call_target="tpu_custom_call" | custom-call | tf_op jit(solution)/shard_map/pallas_call | solution.py:647
  51.6 0.8 %copy.9 = bf16[128,2048]{1,0:T(8,128)(2,1)} copy(bf16[128,2048]{1,0:T(8,128)(2,1)S(1)} %shard_map.73) | data formatting | bytes 1048576

commit v6 on v5

--- a/solution.py
+++ b/solution.py
@@ -55,6 +55,7 @@
 EARLY = 1
 AHEAD = 3
 DIRECT = 3
+PACED = 4
 GROUPS = ((0, 1), (1, 3), (3, 8))
 DENSE_BY = ((0, 2, 3, 4, 5, 6, 7, 8), (0, 1, 2, 3, 4, 5, 6, 7, 8))
 EDENSE_BY = (0, 4, 6, 8)
@@ -407,11 +408,11 @@
                 for j in crossing[:tp_count - at_relay]:
                     if not at_relay and (c, j) in to_hop and v == 0:
                         to_hop[c, j].start()
-                    elif at_relay or v or c <= DIRECT:
+                    elif v or c <= (PACED if at_relay else DIRECT):
                         far_ret[v, c, j].start()
 
-    def late_return(c):
-        for j in crossing[side:]:
+    def late_return(c, js=None):
+        for j in crossing[side:] if js is None else js:
             far_ret[0, c, j].start()
 
     def hop_on(c):
@@ -526,6 +527,8 @@
         relay_out(1, 6)
         relay_back(0, 1)
         relay_out(1, 7)
+        for c in range(PACED + 1, PIECES):
+            late_return(c, crossing[:-1])
 
         @pl.when(jnp.logical_not(is_first))
         def _():
@@ -541,14 +544,16 @@
 
         relay_back(0, 2)
         relay_back(0, 3)
-        for c in range(4):
+        for c in range(last):
             far_in(1, c, 1)
         relay_back(0, 4)
-        for c in range(4, PIECES):
-            far_in(1, c, 1)
+        far_in(1, last, 1)
         far_result(1, 1)
         relay_back(0, 5)
-        relay_back(0, last - 1)
+
+        @pl.when(jnp.logical_not(jnp.logical_and(holds_back, tp % 2 == 0)))
+        def _():
+            relay_back(0, last - 1)
 
         @pl.when(jnp.logical_not(holds_back))
         def _():
@@ -556,6 +561,10 @@
 
         for c in range(PIECES):
             relay_back(1, c)
+
+        @pl.when(jnp.logical_and(holds_back, tp % 2 == 0))
+        def _():
+            relay_back(0, last - 1)
 
         @pl.when(holds_back)
         def _():

time: 52.5 us -> 52.2 us (level)
  Pallas kernels: 51.6 us -> 51 us
    pallas_call x1, Pallas kernels: 51.6 us -> 51 us  [fused(): pl.pallas_call(functools.partial(kernel, ep_count, tp_count, cap), out_sh...]
where the time goes in v6:
time: 52.2 us; the launch traced here: 51.8 us
  Pallas kernels  51 us (98%)
  local copies, waits for them, and re-layouts  0.8 us (2%)
    pallas_call x1, Pallas kernels, fused(): pl.pallas_call(functools.partial(kernel, ep_count, tp_count, cap), out_sh...  51 us

profile of v6, /device:TPU:0, one launch (start us, length us, event | category | flops | bytes accessed | tf_op | source)
XLA Modules:
  0.0 51.8 jit_solution(17780404745519131840)
XLA Ops:
  0.0 51.0 %shard_map.73 = bf16[128,2048]{1,0:T(8,128)(2,1)S(1)} custom-call(bf16[128,2048]{1,0:T(8,128)(2,1)} %x_hbm.1, f32[1,2048]{1,0:T(1,128)} %bitcast.3, s32[2,128]{1,0:T(2,128)} %bitcast.4, f32[2,128]{1,0:T(2,128)} %bitcast.5, bf16[1,2048,512]{2,1,0:T(8,128)(2,1)} %wg_hbm.1, bf16[1,2048,512]{2,1,0:T(8,128)(2,1)} %wu_hbm.1, bf16[1,512,2048]{2,1,0:T(8,128)(2,1)} %wd_hbm.1), custom_call_target="tpu_custom_call" | custom-call | tf_op jit(solution)/shard_map/pallas_call | solution.py:656
  51.0 0.8 %copy.9 = bf16[128,2048]{1,0:T(8,128)(2,1)} copy(bf16[128,2048]{1,0:T(8,128)(2,1)S(1)} %shard_map.73) | data formatting | bytes 1048576

commit v7 on v6

--- a/solution.py
+++ b/solution.py
@@ -55,7 +55,7 @@
 EARLY = 1
 AHEAD = 3
 DIRECT = 3
-PACED = 4
+PACED = 3
 GROUPS = ((0, 1), (1, 3), (3, 8))
 DENSE_BY = ((0, 2, 3, 4, 5, 6, 7, 8), (0, 1, 2, 3, 4, 5, 6, 7, 8))
 EDENSE_BY = (0, 4, 6, 8)
@@ -438,21 +438,31 @@
         rsend[v, c] = combine(rshare_hi[v], rshare_lo[v], block).astype(jnp.bfloat16)
         final[v, c].start()
 
-    def combine_near():
-        for p in range(2):
-            lo = p * half
-            first = p * tp_count + 1 - p
-            drain(nback.at[pl.ds(first, tp_count - 1 + p)], io_sem.at[2 + p])
-            block = nback[p * tp_count:(p + 1) * tp_count].reshape(half, width)
-            part = combine(share_hi[lo:lo + half], share_lo[lo:lo + half], block)
-            acc[...] = acc[...] + part if p else part
-
-    def finish(c):
+    def combine_part(p):
+        lo = p * half
+        first = p * tp_count + 1 - p
+        drain(nback.at[pl.ds(first, tp_count - 1 + p)], io_sem.at[2 + p])
+        block = nback[p * tp_count:(p + 1) * tp_count].reshape(half, width)
+        return combine(share_hi[lo:lo + half], share_lo[lo:lo + half], block)
+
+    def arrived(c):
         g, lo, count = span(FINAL_BY, c)
         if c == lo:
             drain(farback.at[pl.ds(lo, count)], io_sem.at[g])
-        part = acc[:, c * part_w:(c + 1) * part_w] + farback[c].astype(jnp.float32)
-        out_ref[:, c * part_w:(c + 1) * part_w] = part.astype(out_ref.dtype)
+
+    def finish_all():
+        acc[...] = combine_part(0)
+        part = combine_part(1)
+        tail = (PIECES - 1) * part_w
+        for c in range(PIECES - 1):
+            arrived(c)
+            cols = slice(c * part_w, (c + 1) * part_w)
+            total = acc[:, cols] + part[:, cols] + farback[c].astype(jnp.float32)
+            out_ref[:, cols] = total.astype(out_ref.dtype)
+        acc[:, tail:] = acc[:, tail:] + part[:, tail:]
+        arrived(PIECES - 1)
+        total = acc[:, tail:] + farback[PIECES - 1].astype(jnp.float32)
+        out_ref[:, tail:] = total.astype(out_ref.dtype)
 
     others = range(1, tp_count)
     second = range(tp_count, near)
@@ -570,9 +580,7 @@
         def _():
             relay_back(0, last)
 
-        combine_near()
-        for c in range(PIECES):
-            finish(c)
+        finish_all()
 
     @pl.when(is_end)
     def _():
@@ -607,9 +615,7 @@
         return_near(list(second)[EARLY:side])
         near_part(tp_count + side, 0, tp_count - side, 2)
         return_near(list(second)[side:])
-        combine_near()
-        for c in range(PIECES):
-            finish(c)
+        finish_all()
 
     drain(normed, dense_s)
     drain(nres.at[pl.ds(1, near - 1)], w_sem.at[0])

time: 52.2 us -> 52.2 us (level)
  no operation moved by 1% of the time
where the time goes in v7:
time: 52.2 us; the launch traced here: 51.7 us
  Pallas kernels  50.9 us (98%)
  local copies, waits for them, and re-layouts  0.8 us (2%)
    pallas_call x1, Pallas kernels, fused(): pl.pallas_call(functools.partial(kernel, ep_count, tp_count, cap), out_sh...  50.9 us

profile of v7, /device:TPU:0, one launch (start us, length us, event | category | flops | bytes accessed | tf_op | source)
XLA Modules:
  0.0 51.7 jit_solution(7528031996907142710)
XLA Ops:
  0.0 50.9 %shard_map.73 = bf16[128,2048]{1,0:T(8,128)(2,1)S(1)} custom-call(bf16[128,2048]{1,0:T(8,128)(2,1)} %x_hbm.1, f32[1,2048]{1,0:T(1,128)} %bitcast.3, s32[2,128]{1,0:T(2,128)} %bitcast.4, f32[2,128]{1,0:T(2,128)} %bitcast.5, bf16[1,2048,512]{2,1,0:T(8,128)(2,1)} %wg_hbm.1, bf16[1,2048,512]{2,1,0:T(8,128)(2,1)} %wu_hbm.1, bf16[1,512,2048]{2,1,0:T(8,128)(2,1)} %wd_hbm.1), custom_call_target="tpu_custom_call" | custom-call | tf_op jit(solution)/shard_map/pallas_call | solution.py:662
  50.9 0.8 %copy.9 = bf16[128,2048]{1,0:T(8,128)(2,1)} copy(bf16[128,2048]{1,0:T(8,128)(2,1)S(1)} %shard_map.73) | data formatting | bytes 1048576
